TPU v7x, 256 devices: a 4x2x16 block of a 4x16x16 slice. The times are simulated.
256 devices in a mesh: grp: 2 (over y), ep: 64 (over z, x), tp: 2 (over core).
Axes of the slice: x: 4, y: 2, z: 16, core: 2. Of those that a mesh axis runs over, the one named last changes fastest.
The devices are a block of a 4x16x16 slice.
Arguments:
- hidden_state: bfloat16 [8192, 1024], P(('grp', 'ep'), 'tp'), parts along dimension 0, may hold values from -6 to 6
- expert_ids: int32 [8192, 4], P(('grp', 'ep')), parts along dimension 0, may hold values from 0 to 63, all different within a row; in each aligned block of 64 rows (0 to 63, 64 to 127, ...) at most 8 rows name the same one
- route_weight: float32 [8192, 4], P(('grp', 'ep')), parts along dimension 0, may hold values from 0.1 to 1
- gate_matrix: bfloat16 [64, 1024, 2048], P('ep', None, 'tp'), may hold values from -0.1875 to 0.1875
- up_matrix: bfloat16 [64, 1024, 2048], P('ep', None, 'tp'), may hold values from -0.1875 to 0.1875
- down_matrix: bfloat16 [64, 2048, 1024], P('ep', 'tp'), may hold values from -2 to 2
- norm_gain: float32 [1024], P('tp'), may hold values from 0.1 to 1.9
Outputs:
- normed_out: bfloat16 [8192, 1024], P(('grp', 'ep'), 'tp'), parts along dimension 0
There are 2 independent parts, one for each index of `grp`. A program takes and returns all parts, laid end to end along the dimension named above; an argument that names none is the same for every part. Nothing has to cross between parts.
Inputs may be any that keep to these rules, and one draw needn't show every extreme that they name: `expert_ids`: each row names 4 different experts. Within the rows of one index of ep (aligned blocks of 64 rows) no expert is named by more than 8 rows, and in some blocks one expert is named by exactly 8 rows. Every expert is named by some row.
All inputs are finite; a program needn't handle non-finite values.
Results may differ from a plain program's by a relative error of at most 0.0065.
Values may be sent and summed in bfloat16 or wider, within the bound.
No kernel may reach another device: no remote copies, remote signals or barrier semaphores. Data moves between devices by JAX's collectives and lax.ppermute only.
A program may use at most 64 MiB of HBM per device.

v0:
```python
import jax
import jax.numpy as jnp
from jax import lax
from jax.sharding import PartitionSpec as P

D = 1024


norm_eps = 1e-05


def in_blocks(array, dim, length):
    before, after = (array.shape[:dim], array.shape[dim + 1 :])
    return jnp.moveaxis(array.reshape(*before, length, -1, *after), dim, 0)


def sum_at_owner(array, axis, dim):
    length = lax.axis_size(axis)
    parts = lax.all_to_all(in_blocks(array, dim, length), axis, 0, 0, tiled=True)
    return jnp.sum(parts.astype(jnp.float32), axis=0)


def laid_out(parts, dim):
    shape = list(parts.shape[1:])
    shape[dim] *= parts.shape[0]
    return jnp.moveaxis(parts, 0, dim).reshape(shape)


def copy_for_each(array, axis):
    length = lax.axis_size(axis)
    return lax.all_to_all(
        jnp.broadcast_to(array[None], (length, *array.shape)), axis, 0, 0, tiled=True
    )


def collect(array, axis, dim):
    return laid_out(copy_for_each(array, axis), dim)


def slot_numbers(block_ids, expert_count):
    onehot = (block_ids[..., None] == jnp.arange(expert_count, dtype=jnp.int32)).astype(jnp.int32)
    earlier = jnp.cumsum(onehot, axis=-2) - onehot
    return jnp.sum(earlier * onehot, axis=-1)


def expert_rows(buffer, gate_matrix, up_matrix, down_matrix):
    sources, item_count, feature_count = buffer.shape
    token_rows = buffer.reshape(sources * item_count, feature_count)
    gate_pre = jnp.dot(token_rows, gate_matrix[0], preferred_element_type=jnp.float32)
    up_pre = jnp.dot(token_rows, up_matrix[0], preferred_element_type=jnp.float32)
    activated = (jax.nn.silu(gate_pre) * up_pre).astype(jnp.bfloat16)
    partial_value = jnp.dot(activated, down_matrix[0], preferred_element_type=jnp.float32)
    summed = sum_at_owner(
        partial_value.reshape(sources, item_count, feature_count).astype(jnp.bfloat16), "tp", 2
    )
    return summed.astype(jnp.bfloat16)


def shards(hidden_state, expert_ids, route_weight, gate_matrix, up_matrix, down_matrix, norm_gain):
    tok_count, top_count = expert_ids.shape
    expert_count = lax.axis_size("ep")
    capacity = max(2, 2 * tok_count * top_count // expert_count)
    slot_total = expert_count * capacity
    slot_rank = slot_numbers(expert_ids.reshape(1, tok_count * top_count), expert_count)
    slot_index = expert_ids * capacity + slot_rank.reshape(tok_count, top_count)
    positions = jnp.arange(slot_total, dtype=jnp.int32)
    matches = slot_index[:, :, None] == positions[None, None, :]
    placing = jnp.transpose(jnp.any(matches, axis=1)).astype(jnp.bfloat16)
    combine = jnp.sum(jnp.where(matches, route_weight[:, :, None], 0.0), axis=1)
    outgoing = jnp.dot(placing, hidden_state, preferred_element_type=jnp.float32).astype(
        jnp.bfloat16
    )
    answers = expert_rows(
        collect(
            lax.all_to_all(
                outgoing.reshape(expert_count, capacity, hidden_state.shape[1]),
                "ep",
                split_axis=0,
                concat_axis=0,
                tiled=True,
            ),
            "tp",
            2,
        ),
        gate_matrix,
        up_matrix,
        down_matrix,
    )
    returned = lax.all_to_all(answers, "ep", split_axis=0, concat_axis=0, tiled=True)
    combined = jnp.dot(
        combine,
        returned.reshape(slot_total, returned.shape[2]).astype(jnp.float32),
        precision=lax.Precision.HIGHEST,
    )
    local_squares = jnp.sum(combined * combined, axis=1)
    total_squares = lax.psum(local_squares, "tp")
    inverse_rms = lax.rsqrt(total_squares / D + norm_eps)
    return (combined * inverse_rms[:, None] * norm_gain).astype(jnp.bfloat16)


def solution(mesh):
    placed = (
        P(("grp", "ep"), "tp"),
        P(("grp", "ep"), None),
        P(("grp", "ep"), None),
        P("ep", None, "tp"),
        P("ep", None, "tp"),
        P("ep", "tp", None),
        P("tp"),
    )
    return jax.shard_map(
        shards, mesh=mesh, in_specs=placed, out_specs=P(("grp", "ep"), "tp"), check_vma=False
    )
```

profile of v0, /device:TPU:33, one launch (start us, length us, event | category | flops | bytes accessed | tf_op | source)
XLA Modules:
  0.0 130.7 jit_solution(2665535708443496300)
XLA Ops:
  0.0 0.0 copy-start
  0.0 0.9 copy.35
  0.9 0.1 eq.40
  1.0 0.1 compare_convert_fusion
  1.1 0.6 reduce-window.6
  1.7 0.2 slice_reduce_fusion
  1.9 0.1 copy.37
  2.0 0.1 copy.38
  2.1 0.1 broadcast.56
  2.2 0.1 fusion.20
  2.4 0.1 reshape.140
  2.5 0.1 copy.39
  2.6 0.7 multiply_add_fusion
  3.3 0.1 fusion.19
  3.4 1.2 fusion.14
  4.6 58.4 %all_to_all.20 = bf16[64,8,512]{2,1,0:T(8,128)(2,1)S(1)} all-to-all(bf16[64,8,512]{2,1,0:T(8,128)(2,1)S(1)} %fusion.14), channel_id=1, replica_groups=mesh['grp'=2,'ep'=64,'tp'=2] {'ep'}, dimensions={0} | all-to-all | bytes 1048576 | tf_op jit(solution)/shard_map/all_to_all | solution.py:75
  63.0 0.1 broadcast_in_dim.16
  63.0 7.5 %all_to_all.21 = bf16[2,64,8,512]{3,2,1,0:T(8,128)(2,1)S(1)} all-to-all(bf16[2,64,8,512]{3,2,1,0:T(8,128)(2,1)S(1)} %broadcast_in_dim.16), channel_id=1, replica_groups=mesh['grp'=2,'ep'=64,'tp'=2] {'tp'}, dimensions={0} | all-to-all | bytes 2097152 | tf_op jit(solution)/shard_map/all_to_all | solution.py:31
  70.6 1.1 copy.46
  71.7 0.2 copy.42
  71.9 0.0 copy-done
  71.9 2.6 %fusion.4 = f32[512,1024]{1,0:T(8,128)} fusion(bf16[512,1024]{1,0:T(8,128)(2,1)S(1)} %bitcast.60, bf16[1,1024,1024]{2,1,0:T(8,128)(2,1)S(1)} %copy-done), kind=kOutput, calls=%fused_computation.4 | convolution fusion | flops 1073741824 | bytes 5242880 | tf_op jit(solution)/shard_map/dot_general | solution.py:49
  74.5 6.2 %fusion.8 = bf16[64,8,1024]{2,1,0:T(8,128)(2,1)} fusion(bf16[1,1024,1024]{2,1,0:T(8,128)(2,1)} %param.12, bf16[512,1024]{1,0:T(8,128)(2,1)S(1)} %bitcast.61, bf16[1,1024,1024]{2,1,0:T(8,128)(2,1)} %param.11, f32[512,1024]{1,0:T(8,128)} %fusion.4), kind=kOutput, calls=%fused_computation.7 | convolution fusion | flops 2151153664 | bytes 8388608 | tf_op jit(solution)/shard_map/dot_general | solution.py:52
  80.8 1.3 copy.45
  82.1 0.0 copy-start.1
  82.1 4.6 %all_to_all.22 = bf16[2,64,8,512]{3,2,1,0:T(8,128)(2,1)S(1)} all-to-all(bf16[2,64,8,512]{3,2,1,0:T(8,128)(2,1)S(1)} %bitcast.59), channel_id=1, replica_groups=mesh['grp'=2,'ep'=64,'tp'=2] {'tp'}, dimensions={0} | all-to-all | bytes 2097152 | tf_op jit(solution)/shard_map/all_to_all | solution.py:19
  86.7 0.0 copy-start.2
  86.7 1.1 reduce_sum.41
  87.8 7.2 %all-to-all-start.3 = ((bf16[64,8,512]{2,1,0:T(8,128)(2,1)}), bf16[64,8,512]{2,1,0:T(8,128)(2,1)S(1)}, u32[]{:S(2)}, u32[]{:S(2)}) async-start(bf16[64,8,512]{2,1,0:T(8,128)(2,1)} %reduce_sum.41), calls=%async_computation.3 | async-start | bytes 1048576 | tf_op jit(solution)/shard_map/all_to_all | solution.py:89
  95.0 0.0 copy-done.1
  95.0 0.1 select_reduce_fusion
  95.1 29.4 %all-to-all-done.3 = bf16[64,8,512]{2,1,0:T(8,128)(2,1)S(1)} async-done(((bf16[64,8,512]{2,1,0:T(8,128)(2,1)}), bf16[64,8,512]{2,1,0:T(8,128)(2,1)S(1)}, u32[]{:S(2)}, u32[]{:S(2)}) %all-to-all-start.3) | async-done | bytes 524320 | tf_op jit(solution)/shard_map/all_to_all | solution.py:89
  124.5 0.5 multiply_reduce_fusion
  125.0 5.0 %psum.7 = f32[64]{0:T(128)S(1)} all-reduce(f32[64]{0:T(128)S(1)} %get-tuple-element.5), channel_id=1, replica_groups=mesh['grp'=2,'ep'=64,'tp'=2] {'tp'}, use_global_device_ids=true, to_apply=%region_7.8 | all-reduce | flops 64 | bytes 512 | tf_op jit(solution)/shard_map/psum | solution.py:96
  129.9 0.0 copy-done.2
  129.9 0.7 multiply_convert_fusion.1
  (4 shorter events, 0.1 us)
Async XLA Ops:
  0.0 71.9 %copy-start = (bf16[1,1024,1024]{2,1,0:T(8,128)(2,1)S(1)}, bf16[1,1024,1024]{2,1,0:T(8,128)(2,1)}, u32[]{:S(2)}) copy-start(bf16[1,1024,1024]{2,1,0:T(8,128)(2,1)} %param.10) | copy-start | bytes 6291460
  82.1 12.9 %copy-start.1 = (f32[64,4]{0,1:T(4,128)S(1)}, f32[64,4]{0,1:T(4,128)}, u32[]{:S(2)}) copy-start(f32[64,4]{0,1:T(4,128)} %param.9) | copy-start | bytes 3076
  86.7 43.3 %copy-start.2 = (f32[512]{0:T(512)S(1)}, f32[512]{0:T(512)}, u32[]{:S(2)}) copy-start(f32[512]{0:T(512)} %param.13) | copy-start | bytes 6148
  87.8 36.7 %all-to-all-start.3 = ((bf16[64,8,512]{2,1,0:T(8,128)(2,1)}), bf16[64,8,512]{2,1,0:T(8,128)(2,1)S(1)}, u32[]{:S(2)}, u32[]{:S(2)}) async-start(bf16[64,8,512]{2,1,0:T(8,128)(2,1)} %reduce_sum.41), calls=%async_computation.3 | async-start | bytes 1048576 | tf_op jit(solution)/shard_map/all_to_all | solution.py:89
where the time goes:
time: 131 us
  blocking collectives  75.4 us (58%)
  waiting for transfers between devices  29.4 us (22%)
  matrix products  10.5 us (8%)
  starting transfers between devices  7.18 us (5%)
  local copies, waits for them, and re-layouts  4.38 us (3%)
  other arithmetic  3.66 us (3%)
    all_to_all x1, blocking collectives, shards(): lax.all_to_all(outgoing.reshape(expert_count, capacity, hidden_state.shap...  58.4 us
    all_to_all x1, waiting for transfers between devices, shards(): lax.all_to_all(answers, 'ep', split_axis=0, concat_axis=0, tiled=True)  29.4 us
    all_to_all x1, blocking collectives, copy_for_each(): lax.all_to_all(jnp.broadcast_to(array[None], (length, *array.shape)), axi...  7.54 us
    all_to_all x1, starting transfers between devices, shards(): lax.all_to_all(answers, 'ep', split_axis=0, concat_axis=0, tiled=True)  7.18 us
    dot_general x1, matrix products, expert_rows(): jnp.dot(activated, down_matrix[0], preferred_element_type=jnp.float32)  6.21 us
    psum x1, blocking collectives, shards(): total_squares = lax.psum(local_squares, 'tp')  4.96 us
    all_to_all x1, blocking collectives, sum_at_owner(): lax.all_to_all(in_blocks(array, dim, length), axis, 0, 0, tiled=True)  4.58 us
    dot_general x1, matrix products, expert_rows(): jnp.dot(token_rows, gate_matrix[0], preferred_element_type=jnp.float32)  2.62 us
  transfers between devices with their start and end apart: 1, of which 1 were waited for; matrix products, arithmetic and copies ran while one was open for 0% of the time, Pallas kernels for 0%

commit v1 on v0

v1 whole, which is shorter than its diff:
```python
import functools

import jax
import jax.numpy as jnp
from jax import lax
from jax.experimental import pallas as pl
from jax.experimental.pallas import tpu as pltpu
from jax.sharding import PartitionSpec as P

norm_eps = 1e-05
f32, bf16, i32 = jnp.float32, jnp.bfloat16, jnp.int32


def dot(a, b, dims=((1,), (0,))):
    return lax.dot_general(a, b, (dims, ((), ())), preferred_element_type=f32)


def iota(shape, dim):
    return lax.broadcasted_iota(i32, shape, dim)


def slot_ranks(ids, expert_count):
    rows, top = ids.shape
    lanes = iota((rows, expert_count), 1)
    named = ids[:, 0:1] == lanes
    for k in range(1, top):
        named = named | (ids[:, k : k + 1] == lanes)
    named = jnp.where(named, 1.0, 0.0)
    earlier = jnp.where(iota((rows, rows), 1) < iota((rows, rows), 0), 1.0, 0.0)
    return named, dot(earlier.astype(bf16), named.astype(bf16))


def pack_body(ids_ref, hidden_ref, out_ref, *, expert_count, capacity):
    named, rank = slot_ranks(ids_ref[...], expert_count)
    code = jnp.where(named > 0, rank, -1.0).astype(bf16)
    slots = expert_count * capacity
    spread = iota((slots, expert_count), 0) // capacity == iota((slots, expert_count), 1)
    spread = jnp.where(spread, 1.0, 0.0).astype(bf16)
    wanted = dot(spread, code, ((1,), (1,)))
    own = (iota(wanted.shape, 0) % capacity).astype(f32)
    placing = jnp.where(wanted == own, 1.0, 0.0).astype(bf16)
    out_ref[...] = dot(placing, hidden_ref[...]).astype(bf16)


def pack(ids, hidden, expert_count, capacity):
    body = functools.partial(pack_body, expert_count=expert_count, capacity=capacity)
    return pl.pallas_call(
        body,
        out_shape=jax.ShapeDtypeStruct((expert_count * capacity, hidden.shape[1]), bf16),
        name="pack",
    )(ids, hidden)


def hidden_body(tp_ref, own_ref, other_ref, gate_ref, up_ref, down_ref, act_ref, send_ref, acc_ref):
    step = pl.program_id(0)
    half = own_ref.shape[1]
    mine = pl.multiple_of(tp_ref[0] * half, half)
    theirs = pl.multiple_of((1 - tp_ref[0]) * half, half)
    own, other = own_ref[...], other_ref[...]
    gate = dot(own, gate_ref[0, pl.ds(mine, half), :]) + dot(other, gate_ref[0, pl.ds(theirs, half), :])
    up = dot(own, up_ref[0, pl.ds(mine, half), :]) + dot(other, up_ref[0, pl.ds(theirs, half), :])
    act = (gate / (1.0 + jnp.exp(-gate)) * up).astype(bf16)
    act_ref[...] = act
    part = dot(act, down_ref[0])

    @pl.when(step == 0)
    def _():
        acc_ref[...] = part

    @pl.when(step > 0)
    def _():
        acc_ref[...] += part

    @pl.when(step == pl.num_programs(0) - 1)
    def _():
        send_ref[...] = acc_ref[...].astype(bf16)


def hidden_part(tp, own, other, gate, up, down, tile=256):
    rows, half = own.shape
    width, units = gate.shape[1:]
    whole = pl.BlockSpec((rows, half), lambda j, t: (0, 0))
    return pl.pallas_call(
        hidden_body,
        grid_spec=pltpu.PrefetchScalarGridSpec(
            num_scalar_prefetch=1,
            grid=(units // tile,),
            in_specs=[
                whole,
                whole,
                pl.BlockSpec((1, width, tile), lambda j, t: (0, 0, j)),
                pl.BlockSpec((1, width, tile), lambda j, t: (0, 0, j)),
                pl.BlockSpec((1, tile, half), lambda j, t: (0, j, 1 - t[0])),
            ],
            out_specs=[pl.BlockSpec((rows, tile), lambda j, t: (0, j)), whole],
            scratch_shapes=[pltpu.VMEM((rows, half), f32)],
        ),
        out_shape=[jax.ShapeDtypeStruct((rows, units), bf16), jax.ShapeDtypeStruct((rows, half), bf16)],
        cost_estimate=pl.CostEstimate(
            flops=2 * rows * units * (2 * width + half), bytes_accessed=2 * units * (2 * width + half), transcendentals=rows * units
        ),
        name="hidden_part",
    )(tp, own, other, gate, up, down)


def keep_body(tp_ref, act_ref, down_ref, out_ref):
    out_ref[...] = dot(act_ref[...], down_ref[0]).astype(bf16)


def keep_part(tp, act, down, half):
    rows, units = act.shape
    return pl.pallas_call(
        keep_body,
        grid_spec=pltpu.PrefetchScalarGridSpec(
            num_scalar_prefetch=1,
            grid=(1,),
            in_specs=[
                pl.BlockSpec((rows, units), lambda j, t: (0, 0)),
                pl.BlockSpec((1, units, half), lambda j, t: (0, 0, t[0])),
            ],
            out_specs=pl.BlockSpec((rows, half), lambda j, t: (0, 0)),
        ),
        out_shape=jax.ShapeDtypeStruct((rows, half), bf16),
        cost_estimate=pl.CostEstimate(flops=2 * rows * units * half, bytes_accessed=2 * units * half, transcendentals=0),
        name="keep_part",
    )(tp, act, down)


def combine_body(ids_ref, weight_ref, back_ref, out_ref, square_ref, *, expert_count, capacity):
    ids = ids_ref[...]
    rows, top = ids.shape
    _, rank = slot_ranks(ids, expert_count)
    lanes = iota((rows, expert_count), 1)
    places = iota((rows, expert_count * capacity), 1)
    weights = jnp.zeros(places.shape, f32)
    for k in range(top):
        column = ids[:, k : k + 1]
        at = jnp.sum(jnp.where(column == lanes, rank, 0.0), axis=1, keepdims=True).astype(i32)
        weights += jnp.where(column * capacity + at == places, weight_ref[:, k : k + 1], 0.0)
    high = weights.astype(bf16)
    low = (weights - high.astype(f32)).astype(bf16)
    back = back_ref[...]
    combined = dot(high, back) + dot(low, back)
    out_ref[...] = combined
    square_ref[...] = jnp.broadcast_to(jnp.sum(combined * combined, axis=1, keepdims=True), square_ref.shape)


def combine(ids, weights, back, expert_count, capacity):
    rows = ids.shape[0]
    body = functools.partial(combine_body, expert_count=expert_count, capacity=capacity)
    return pl.pallas_call(
        body,
        out_shape=[jax.ShapeDtypeStruct((rows, back.shape[1]), f32), jax.ShapeDtypeStruct((rows, 128), f32)],
        name="combine",
    )(ids, weights, back)


def shards(hidden_state, expert_ids, route_weight, gate_matrix, up_matrix, down_matrix, norm_gain):
    tok_count, top_count = expert_ids.shape
    half = hidden_state.shape[1]
    experts = lax.axis_size("ep")
    capacity = max(2, 2 * tok_count * top_count // experts)
    tp = lax.axis_index("tp").reshape(1)
    swap = lambda a: lax.ppermute(a, "tp", [(0, 1), (1, 0)])
    exchange = lambda a: lax.all_to_all(a.reshape(experts, capacity, half), "ep", 0, 0, tiled=True).reshape(
        experts * capacity, half
    )
    own = exchange(pack(expert_ids, hidden_state, experts, capacity))
    act, send = hidden_part(tp, own, swap(own), gate_matrix, up_matrix, down_matrix)
    got = swap(send)
    kept = keep_part(tp, act, down_matrix, half)
    answers = (kept.astype(f32) + got.astype(f32)).astype(bf16)
    combined, squares = combine(expert_ids, route_weight, exchange(answers), experts, capacity)
    total = (squares + swap(squares))[:, :1]
    width = half * lax.axis_size("tp")
    return (combined * lax.rsqrt(total / width + norm_eps) * norm_gain).astype(bf16)


def solution(mesh):
    placed = (
        P(("grp", "ep"), "tp"),
        P(("grp", "ep"), None),
        P(("grp", "ep"), None),
        P("ep", None, "tp"),
        P("ep", None, "tp"),
        P("ep", "tp", None),
        P("tp"),
    )
    return jax.shard_map(
        shards, mesh=mesh, in_specs=placed, out_specs=P(("grp", "ep"), "tp"), check_vma=False
    )
```

time: 131 us -> 127 us (0.969)
  blocking collectives: 75.4 us -> 58.6 us
  Pallas kernels: 0 us -> 14.9 us
  matrix products: 10.5 us -> 0 us
  starting transfers between devices: 7.18 us -> 13.3 us
  waiting for transfers between devices: 29.4 us -> 31.8 us
    pallas_call x0 -> x4, Pallas kernels: none -> 14.9 us  [the longest x1 7.1 us: hidden_part(): pl.pallas_call(hidden_body, grid_spec=pltpu.PrefetchScalarGridSpec(num_sc...]
    all_to_all x3 -> x1, blocking collectives: 70.5 us -> 58.6 us  [shards(): lax.all_to_all(a.reshape(experts, capacity, half), 'ep', 0, 0, tiled=True)]
    dot_general x4 -> x0, matrix products: 10.5 us -> none  [the longest x1 6.21 us: expert_rows(): jnp.dot(activated, down_matrix[0], preferred_element_type=jnp.float32)]
    ppermute x0 -> x3, starting transfers between devices: none -> 6.1 us  [shards(): swap = lambda a: lax.ppermute(a, 'tp', [(0, 1), (1, 0)])]
    psum x1 -> x0, blocking collectives: 4.96 us -> none  [shards(): total_squares = lax.psum(local_squares, 'tp')]
    ppermute x0 -> x3, waiting for transfers between devices: none -> 2.61 us  [shards(): swap = lambda a: lax.ppermute(a, 'tp', [(0, 1), (1, 0)])]
    unnamed x8 -> x12, local copies, waits for them, and re-layouts: 1.18 us -> 3.69 us
    reshape x0 -> x1, other arithmetic: none -> 1.99 us  [shards(): a.reshape(experts, capacity, half)]
  transfers between devices with their start and end apart: 1 -> 4, of which waited for: 1 -> 3; matrix products, arithmetic and copies ran while one was open for 0% -> 1% of each run, Pallas kernels for 0% -> 2%
where the time goes in v1:
time: 127 us
  blocking collectives  58.6 us (46%)
  waiting for transfers between devices  31.8 us (25%)
  Pallas kernels  14.9 us (12%)
  starting transfers between devices  13.3 us (10%)
  other arithmetic  4.48 us (4%)
  local copies, waits for them, and re-layouts  3.69 us (3%)
    all_to_all x1, blocking collectives, shards(): lax.all_to_all(a.reshape(experts, capacity, half), 'ep', 0, 0, tiled=True)  58.6 us
    all_to_all x1, waiting for transfers between devices, shards(): lax.all_to_all(a.reshape(experts, capacity, half), 'ep', 0, 0, tiled=True)  29.2 us
    all_to_all x1, starting transfers between devices, shards(): lax.all_to_all(a.reshape(experts, capacity, half), 'ep', 0, 0, tiled=True)  7.17 us
    pallas_call x1, Pallas kernels, hidden_part(): pl.pallas_call(hidden_body, grid_spec=pltpu.PrefetchScalarGridSpec(num_sc...  7.1 us
    ppermute x3, starting transfers between devices, shards(): swap = lambda a: lax.ppermute(a, 'tp', [(0, 1), (1, 0)])  6.1 us
    unnamed x12, local copies, waits for them, and re-layouts  3.69 us
    pallas_call x1, Pallas kernels, keep_part(): pl.pallas_call(keep_body, grid_spec=pltpu.PrefetchScalarGridSpec(num_scal...  3.03 us
    ppermute x3, waiting for transfers between devices, shards(): swap = lambda a: lax.ppermute(a, 'tp', [(0, 1), (1, 0)])  2.61 us
  transfers between devices with their start and end apart: 4, of which 3 were waited for; matrix products, arithmetic and copies ran while one was open for 1% of the time, Pallas kernels for 2%

profile of v1, /device:TPU:33, one launch (start us, length us, event | category | flops | bytes accessed | tf_op | source)
XLA Modules:
  0.0 126.8 jit_solution(7373657642363466189)
XLA Ops:
  0.0 1.4 %copy.12.ids_ref = s32[64,4]{1,0:T(8,128)} copy(s32[64,4]{0,1:T(4,128)} %param.8) | data formatting | bytes 2048 | tf_op args[1]
  1.4 2.3 %pack.1 = bf16[512,512]{1,0:T(8,128)(2,1)} custom-call(s32[64,4]{1,0:T(8,128)} %copy.12.ids_ref, bf16[64,512]{1,0:T(8,128)(2,1)} %hidden_ref.1), custom_call_target="tpu_custom_call" | custom-call | tf_op jit(solution)/shard_map/pack/pallas_call | solution.py:47
  3.7 58.6 %all_to_all.10 = bf16[64,8,512]{2,1,0:T(8,128)(2,1)S(1)} all-to-all(bf16[64,8,512]{2,1,0:T(8,128)(2,1)} %bitcast.7), channel_id=1, replica_groups=mesh['grp'=2,'ep'=64,'tp'=2] {'ep'}, dimensions={0} | all-to-all | bytes 1048576 | tf_op jit(solution)/shard_map/all_to_all | solution.py:165
  62.3 0.0 copy-start.1
  62.3 3.3 %collective-permute-start = (bf16[512,512]{1,0:T(8,128)(2,1)S(1)}, bf16[512,512]{1,0:T(8,128)(2,1)S(1)}, u32[]{:S(2)}, u32[]{:S(2)}) collective-permute-start(bf16[512,512]{1,0:T(8,128)(2,1)S(1)} %bitcast.8), channel_id=1, source_target_pairs={{0,1},{1,0},{2,3},{3,2},{4,5},{5,4},{6,7},{7,6},{8,9},{9,8},{10,11... | collective-permute-start | bytes 1572872 | tf_op jit(solution)/shard_map/ppermute | solution.py:164
  65.6 1.5 %collective-permute-done.other_ref = bf16[512,512]{1,0:T(8,128)(2,1)S(1)} collective-permute-done((bf16[512,512]{1,0:T(8,128)(2,1)S(1)}, bf16[512,512]{1,0:T(8,128)(2,1)S(1)}, u32[]{:S(2)}, u32[]{:S(2)}) %collective-permute-start) | collective-permute-done | bytes 524320 | tf_op jit(solution)/shard_map/ppermute | solution.py:164
  67.1 0.0 copy-start.4
  67.1 0.0 copy-done.1
  67.1 0.8 copy-done.4
  67.9 7.1 %hidden_part.1 = (bf16[512,1024]{1,0:T(8,128)(2,1)}, bf16[512,512]{1,0:T(8,128)(2,1)}) custom-call(s32[1]{0:T(128)} %bitcast.tp_ref, bf16[512,512]{1,0:T(8,128)(2,1)} %bitcast.9, bf16[512,512]{1,0:T(8,128)(2,1)} %copy-done.4, bf16[1,1024,1024]{2,1,0:T(8,128)(2,1)} %gate_ref.1, bf16[1,1024,1024]{2,1,0:T(8,128)(2,1)} %up_ref.1, bf16[1,1024,1024]{2,1,0:T(8,128)(2,1)} %down_ref.3), custom_call_target="tpu_custom_call" | custom-call | flops 2684354560 | bytes 5242880 | tf_op jit(solution)/shard_map/hidden_part/pallas_call | solution.py:83
  75.0 0.4 collective-permute-start.1
  75.4 3.0 %keep_part.1 = bf16[512,512]{1,0:T(8,128)(2,1)} custom-call(s32[1]{0:T(128)} %bitcast.tp_ref, bf16[512,1024]{1,0:T(8,128)(2,1)} %get-tuple-element.9.act_ref, bf16[1,1024,1024]{2,1,0:T(8,128)(2,1)} %down_ref.3), custom_call_target="tpu_custom_call" | custom-call | flops 536870912 | bytes 1048576 | tf_op jit(solution)/shard_map/keep_part/pallas_call | solution.py:112
  78.4 0.0 copy-start.3
  78.4 0.0 copy-start.2
  78.5 0.0 collective-permute-done.1
  78.5 2.0 %fusion = bf16[64,8,512]{2,1,0:T(8,128)(2,1)} fusion(bf16[512,512]{1,0:T(8,128)(2,1)S(1)} %collective-permute-done.1, bf16[512,512]{1,0:T(8,128)(2,1)} %keep_part.1), kind=kLoop, calls=%fused_computation.1 | loop fusion | flops 1048576 | bytes 1572864 | tf_op jit(solution)/shard_map/reshape | solution.py:165
  80.4 7.2 %all-to-all-start.1 = ((bf16[64,8,512]{2,1,0:T(8,128)(2,1)}), bf16[64,8,512]{2,1,0:T(8,128)(2,1)S(1)}, u32[]{:S(2)}, u32[]{:S(2)}) async-start(bf16[64,8,512]{2,1,0:T(8,128)(2,1)} %fusion), calls=%async_computation.1 | async-start | bytes 1048576 | tf_op jit(solution)/shard_map/all_to_all | solution.py:165
  87.6 0.0 copy-done.3
  87.6 0.7 copy.13.weight_ref
  88.3 29.2 %all-to-all-done.1 = bf16[64,8,512]{2,1,0:T(8,128)(2,1)S(1)} async-done(((bf16[64,8,512]{2,1,0:T(8,128)(2,1)}), bf16[64,8,512]{2,1,0:T(8,128)(2,1)S(1)}, u32[]{:S(2)}, u32[]{:S(2)}) %all-to-all-start.1) | async-done | bytes 524320 | tf_op jit(solution)/shard_map/all_to_all | solution.py:165
  117.5 0.0 copy-start
  117.5 0.8 copy-done
  118.3 2.5 %combine.1 = (f32[64,512]{1,0:T(8,128)}, f32[64,128]{1,0:T(8,128)}) custom-call(s32[64,4]{1,0:T(8,128)} %copy.12.ids_ref, f32[64,4]{1,0:T(8,128)} %copy.13.weight_ref, bf16[512,512]{1,0:T(8,128)(2,1)} %bitcast.6), custom_call_target="tpu_custom_call" | custom-call | tf_op jit(solution)/shard_map/combine/pallas_call | solution.py:151
  120.8 2.4 %collective-permute-start.2 = (f32[64,128]{1,0:T(8,128)}, f32[64,128]{1,0:T(8,128)S(1)}, u32[]{:S(2)}, u32[]{:S(2)}) collective-permute-start(f32[64,128]{1,0:T(8,128)} %get-tuple-element.12), channel_id=1, source_target_pairs={{0,1},{1,0},{2,3},{3,2},{4,5},{5,4},{6,7},{7,6},{8,9},{9,8},{10,11... | collective-permute-start | bytes 98312 | tf_op jit(solution)/shard_map/ppermute | solution.py:164
  123.2 1.1 collective-permute-done.2
  124.3 0.9 fusion.4
  125.1 0.0 copy-done.2
  125.1 1.6 %multiply_convert_fusion = bf16[64,512]{1,0:T(8,128)(2,1)} fusion(f32[64,512]{1,0:T(8,128)} %get-tuple-element.11, f32[512]{0:T(512)S(1)} %copy-done.2, f32[64]{0:T(128)S(1)} %fusion.4), kind=kLoop, calls=%fused_computation.2 | loop fusion | flops 98304 | bytes 198912 | tf_op jit(solution)/shard_map/convert_element_type | solution.py:176
Async XLA Ops:
  62.3 4.9 %copy-start.1 = (bf16[64,8,512]{2,1,0:T(8,128)(2,1)}, bf16[64,8,512]{2,1,0:T(8,128)(2,1)S(1)}, u32[]{:S(2)}) copy-start(bf16[64,8,512]{2,1,0:T(8,128)(2,1)S(1)} %all_to_all.10) | copy-start | bytes 1572868
  62.3 4.9 %collective-permute-start = (bf16[512,512]{1,0:T(8,128)(2,1)S(1)}, bf16[512,512]{1,0:T(8,128)(2,1)S(1)}, u32[]{:S(2)}, u32[]{:S(2)}) collective-permute-start(bf16[512,512]{1,0:T(8,128)(2,1)S(1)} %bitcast.8), channel_id=1, source_target_pairs={{0,1},{1,0},{2,3},{3,2},{4,5},{5,4},{6,7},{7,6},{8,9},{9,8},{10,11... | collective-permute-start | bytes 1572872 | tf_op jit(solution)/shard_map/ppermute | solution.py:164
  67.1 0.8 copy-start.4
  75.0 3.4 %collective-permute-start.1 = (bf16[512,512]{1,0:T(8,128)(2,1)}, bf16[512,512]{1,0:T(8,128)(2,1)S(1)}, u32[]{:S(2)}, u32[]{:S(2)}) collective-permute-start(bf16[512,512]{1,0:T(8,128)(2,1)} %get-tuple-element.10), channel_id=1, source_target_pairs={{0,1},{1,0},{2,3},{3,2},{4,5},{5,4},{6,7},{7,6},{8,9},{9,8},{10,11... | collective-permute-start | bytes 1572872 | tf_op jit(solution)/shard_map/ppermute | solution.py:164
  78.4 9.2 %copy-start.3 = (f32[64,4]{0,1:T(4,128)S(1)}, f32[64,4]{0,1:T(4,128)}, u32[]{:S(2)}) copy-start(f32[64,4]{0,1:T(4,128)} %param.9) | copy-start | bytes 3076
  78.4 46.7 %copy-start.2 = (f32[512]{0:T(512)S(1)}, f32[512]{0:T(512)}, u32[]{:S(2)}) copy-start(f32[512]{0:T(512)} %param.13) | copy-start | bytes 6148
  80.4 37.1 %all-to-all-start.1 = ((bf16[64,8,512]{2,1,0:T(8,128)(2,1)}), bf16[64,8,512]{2,1,0:T(8,128)(2,1)S(1)}, u32[]{:S(2)}, u32[]{:S(2)}) async-start(bf16[64,8,512]{2,1,0:T(8,128)(2,1)} %fusion), calls=%async_computation.1 | async-start | bytes 1048576 | tf_op jit(solution)/shard_map/all_to_all | solution.py:165
  117.5 0.8 copy-start
  120.8 3.5 %collective-permute-start.2 = (f32[64,128]{1,0:T(8,128)}, f32[64,128]{1,0:T(8,128)S(1)}, u32[]{:S(2)}, u32[]{:S(2)}) collective-permute-start(f32[64,128]{1,0:T(8,128)} %get-tuple-element.12), channel_id=1, source_target_pairs={{0,1},{1,0},{2,3},{3,2},{4,5},{5,4},{6,7},{7,6},{8,9},{9,8},{10,11... | collective-permute-start | bytes 98312 | tf_op jit(solution)/shard_map/ppermute | solution.py:164

commit v2 on v1

v2 whole, which is shorter than its diff:
```python
import functools

import jax
import jax.numpy as jnp
from jax import lax
from jax.experimental import pallas as pl
from jax.experimental.pallas import tpu as pltpu
from jax.sharding import PartitionSpec as P

norm_eps = 1e-05
f32, bf16, i32 = jnp.float32, jnp.bfloat16, jnp.int32
VMEM = pl.BlockSpec(memory_space=pltpu.VMEM)
SMEM = pl.BlockSpec(memory_space=pltpu.SMEM)


def call(body, name, mib, in_specs, out_shape, scratch=(), cost=None):
    return pl.pallas_call(
        body,
        in_specs=in_specs,
        out_specs=jax.tree.map(lambda _: VMEM, out_shape),
        out_shape=out_shape,
        scratch_shapes=scratch,
        cost_estimate=cost,
        compiler_params=pltpu.CompilerParams(vmem_limit_bytes=mib << 20),
        name=name,
    )


def dot(a, b, dims=((1,), (0,))):
    return lax.dot_general(a, b, (dims, ((), ())), preferred_element_type=f32)


def iota(shape, dim):
    return lax.broadcasted_iota(i32, shape, dim)


def slot_ranks(ids, expert_count):
    top, rows = ids.shape
    experts = iota((expert_count, rows), 0)
    named = ids[0:1] == experts
    for k in range(1, top):
        named = named | (ids[k : k + 1] == experts)
    named = jnp.where(named, 1.0, 0.0)
    earlier = jnp.where(iota((rows, rows), 0) < iota((rows, rows), 1), 1.0, 0.0)
    return named, dot(named.astype(bf16), earlier.astype(bf16))


def pack_body(ids_ref, hidden_ref, out_ref, *, expert_count, capacity):
    named, rank = slot_ranks(ids_ref[...], expert_count)
    code = jnp.where(named > 0, rank, -1.0).astype(bf16)
    slots = expert_count * capacity
    spread = iota((slots, expert_count), 0) // capacity == iota((slots, expert_count), 1)
    spread = jnp.where(spread, 1.0, 0.0).astype(bf16)
    wanted = dot(spread, code)
    own = (iota(wanted.shape, 0) % capacity).astype(f32)
    placing = jnp.where(wanted == own, 1.0, 0.0).astype(bf16)
    out_ref[...] = dot(placing, hidden_ref[...]).astype(bf16)


def pack(ids, hidden, expert_count, capacity):
    body = functools.partial(pack_body, expert_count=expert_count, capacity=capacity)
    out = jax.ShapeDtypeStruct((expert_count * capacity, hidden.shape[1]), bf16)
    return call(body, "pack", 4, [VMEM] * 2, out)(ids, hidden)


def hidden_body(tp_ref, own_ref, other_ref, gate_ref, up_ref, down_ref, act_ref, send_ref, *, tile):
    half = own_ref.shape[1]
    units = gate_ref.shape[2]
    mine = pl.multiple_of(tp_ref[0] * half, half)
    theirs = pl.multiple_of((1 - tp_ref[0]) * half, half)
    own, other = own_ref[...], other_ref[...]
    for start in range(0, units, tile):
        at = slice(start, start + tile)
        gate = dot(own, gate_ref[0, pl.ds(mine, half), at]) + dot(other, gate_ref[0, pl.ds(theirs, half), at])
        up = dot(own, up_ref[0, pl.ds(mine, half), at]) + dot(other, up_ref[0, pl.ds(theirs, half), at])
        act_ref[:, at] = (gate / (1.0 + jnp.exp(-gate)) * up).astype(bf16)
    send_ref[...] = dot(act_ref[...], down_ref[0, :, pl.ds(theirs, half)]).astype(bf16)


def hidden_part(tp, own, other, gate, up, down, tile=256):
    rows, half = own.shape
    width, units = gate.shape[1:]
    cost = pl.CostEstimate(
        flops=2 * rows * units * (2 * width + half), bytes_accessed=2 * units * (2 * width + half), transcendentals=rows * units
    )
    out = [jax.ShapeDtypeStruct((rows, units), bf16), jax.ShapeDtypeStruct((rows, half), bf16)]
    body = functools.partial(hidden_body, tile=tile)
    return call(body, "hidden_part", 16, [SMEM] + [VMEM] * 5, out, cost=cost)(tp, own, other, gate, up, down)


def keep_body(tp_ref, act_ref, down_ref, out_ref):
    half = out_ref.shape[1]
    mine = pl.multiple_of(tp_ref[0] * half, half)
    out_ref[...] = dot(act_ref[...], down_ref[0, :, pl.ds(mine, half)]).astype(bf16)


def keep_part(tp, act, down, half):
    rows, units = act.shape
    cost = pl.CostEstimate(flops=2 * rows * units * half, bytes_accessed=2 * units * half, transcendentals=0)
    out = jax.ShapeDtypeStruct((rows, half), bf16)
    return call(keep_body, "keep_part", 8, [SMEM] + [VMEM] * 2, out, cost=cost)(tp, act, down)


def combine_body(ids_ref, weight_ref, back_ref, out_ref, square_ref, *, expert_count, capacity):
    ids = ids_ref[...]
    top, rows = ids.shape
    _, rank = slot_ranks(ids, expert_count)
    experts = iota((expert_count, rows), 0)
    places = iota((expert_count * capacity, rows), 0)
    weights = jnp.zeros(places.shape, f32)
    for k in range(top):
        row = ids[k : k + 1]
        at = jnp.sum(jnp.where(row == experts, rank, 0.0), axis=0, keepdims=True).astype(i32)
        weights += jnp.where(row * capacity + at == places, weight_ref[k : k + 1], 0.0)
    high = weights.astype(bf16)
    low = (weights - high.astype(f32)).astype(bf16)
    back = back_ref[...]
    over = ((0,), (0,))
    combined = dot(high, back, over) + dot(low, back, over)
    out_ref[...] = combined
    square_ref[...] = jnp.broadcast_to(jnp.sum(combined * combined, axis=1, keepdims=True), square_ref.shape)


def combine(ids, weights, back, expert_count, capacity):
    rows = ids.shape[1]
    body = functools.partial(combine_body, expert_count=expert_count, capacity=capacity)
    out = [jax.ShapeDtypeStruct((rows, back.shape[1]), f32), jax.ShapeDtypeStruct((rows, 128), f32)]
    return call(body, "combine", 4, [VMEM] * 3, out)(ids, weights, back)


def norm_body(combined_ref, square_ref, other_ref, gain_ref, out_ref, *, width):
    total = (square_ref[...] + other_ref[...])[:, 0:1]
    out_ref[...] = (combined_ref[...] * lax.rsqrt(total / width + norm_eps) * gain_ref[...]).astype(bf16)


def norm(combined, squares, others, gain, width):
    body = functools.partial(norm_body, width=width)
    out = jax.ShapeDtypeStruct(combined.shape, bf16)
    return call(body, "norm", 4, [VMEM] * 4, out)(combined, squares, others, gain.reshape(1, -1))


def shards(hidden_state, expert_ids, route_weight, gate_matrix, up_matrix, down_matrix, norm_gain):
    tok_count, top_count = expert_ids.shape
    half = hidden_state.shape[1]
    experts = lax.axis_size("ep")
    capacity = max(2, 2 * tok_count * top_count // experts)
    tp = lax.axis_index("tp").reshape(1)
    ids, weights = expert_ids.T, route_weight.T
    swap = lambda a: lax.ppermute(a, "tp", [(0, 1), (1, 0)])
    exchange = lambda a: lax.all_to_all(a.reshape(experts, capacity, half), "ep", 0, 0, tiled=True).reshape(
        experts * capacity, half
    )
    own = exchange(pack(ids, hidden_state, experts, capacity))
    act, send = hidden_part(tp, own, swap(own), gate_matrix, up_matrix, down_matrix)
    got = swap(send)
    kept = keep_part(tp, act, down_matrix, half)
    answers = (kept.astype(f32) + got.astype(f32)).astype(bf16)
    combined, squares = combine(ids, weights, exchange(answers), experts, capacity)
    return norm(combined, squares, swap(squares), norm_gain, half * lax.axis_size("tp"))


def solution(mesh):
    placed = (
        P(("grp", "ep"), "tp"),
        P(("grp", "ep"), None),
        P(("grp", "ep"), None),
        P("ep", None, "tp"),
        P("ep", None, "tp"),
        P("ep", "tp", None),
        P("tp"),
    )
    return jax.shard_map(
        shards, mesh=mesh, in_specs=placed, out_specs=P(("grp", "ep"), "tp"), check_vma=False
    )
```

time: 127 us -> 117 us (0.921)
  blocking collectives: 58.6 us -> 94.9 us
  waiting for transfers between devices: 31.8 us -> 3.18 us
  Pallas kernels: 14.9 us -> 5.54 us
  starting transfers between devices: 13.3 us -> 6.68 us
  other arithmetic: 4.48 us -> 0.14 us
  local copies, waits for them, and re-layouts: 3.69 us -> 6.31 us
    all_to_all x1 -> x2, blocking collectives: 58.6 us -> 94.9 us  [shards(): lax.all_to_all(a.reshape(experts, capacity, half), 'ep', 0, 0, tiled=True)]
    all_to_all x1 -> x0, waiting for transfers between devices: 29.2 us -> none  [shards(): lax.all_to_all(a.reshape(experts, capacity, half), 'ep', 0, 0, tiled=True)]
    pallas_call x4 -> x5, Pallas kernels: 14.9 us -> 5.54 us  [the longest x1 2.96 us: hidden_part(): call(body, 'hidden_part', 16, [SMEM] + [VMEM] * 5, out, cost=cost)]
    all_to_all x1 -> x0, starting transfers between devices: 7.17 us -> none  [shards(): lax.all_to_all(a.reshape(experts, capacity, half), 'ep', 0, 0, tiled=True)]
    unnamed x12 -> x16, local copies, waits for them, and re-layouts: 3.69 us -> 6.31 us
    reshape x1, other arithmetic: 1.99 us -> 0.14 us  [shards(): a.reshape(experts, capacity, half)]
    convert_element_type x1 -> x0, other arithmetic: 1.62 us -> none  [shards(): (combined * lax.rsqrt(total / width + norm_eps) * norm_gain).astype(bf16)]
  transfers between devices with their start and end apart: 4 -> 3, of which waited for: 3 -> 3; matrix products, arithmetic and copies ran while one was open for 1% -> 0% of each run, Pallas kernels for 2% -> 1%
where the time goes in v2:
time: 117 us
  blocking collectives  94.9 us (81%)
  starting transfers between devices  6.68 us (6%)
  local copies, waits for them, and re-layouts  6.31 us (5%)
  Pallas kernels  5.54 us (5%)
  waiting for transfers between devices  3.18 us (3%)
    all_to_all x2, blocking collectives, shards(): lax.all_to_all(a.reshape(experts, capacity, half), 'ep', 0, 0, tiled=True)  94.9 us
    ppermute x3, starting transfers between devices, shards(): swap = lambda a: lax.ppermute(a, 'tp', [(0, 1), (1, 0)])  6.68 us
    unnamed x16, local copies, waits for them, and re-layouts  6.31 us
    ppermute x3, waiting for transfers between devices, shards(): swap = lambda a: lax.ppermute(a, 'tp', [(0, 1), (1, 0)])  3.18 us
    pallas_call x1, Pallas kernels, hidden_part(): call(body, 'hidden_part', 16, [SMEM] + [VMEM] * 5, out, cost=cost)  2.96 us
  transfers between devices with their start and end apart: 3, of which 3 were waited for; matrix products, arithmetic and copies ran while one was open for 0% of the time, Pallas kernels for 1%

profile of v2, /device:TPU:33, one launch (start us, length us, event | category | flops | bytes accessed | tf_op | source)
XLA Modules:
  0.0 116.8 jit_solution(15549912974012044311)
XLA Ops:
  0.0 0.0 copy-start.1
  0.0 0.8 copy-done.1
  0.8 0.0 copy-start.2
  0.8 0.7 copy-done.2
  1.5 0.5 pack.1
  2.1 58.4 %all_to_all.10 = bf16[64,8,512]{2,1,0:T(8,128)(2,1)S(1)} all-to-all(bf16[64,8,512]{2,1,0:T(8,128)(2,1)S(1)} %bitcast.10), channel_id=1, replica_groups=mesh['grp'=2,'ep'=64,'tp'=2] {'ep'}, dimensions={0} | all-to-all | bytes 1048576 | tf_op jit(solution)/shard_map/all_to_all | solution.py:150
  60.4 3.3 %collective-permute-start = (bf16[512,512]{1,0:T(8,128)(2,1)S(1)}, bf16[512,512]{1,0:T(8,128)(2,1)S(1)}, u32[]{:S(2)}, u32[]{:S(2)}) collective-permute-start(bf16[512,512]{1,0:T(8,128)(2,1)S(1)} %bitcast.11), channel_id=1, source_target_pairs={{0,1},{1,0},{2,3},{3,2},{4,5},{5,4},{6,7},{7,6},{8,9},{9,8},{10,11... | collective-permute-start | bytes 1572872 | tf_op jit(solution)/shard_map/ppermute | solution.py:149
  63.7 1.5 %collective-permute-done.other_ref = bf16[512,512]{1,0:T(8,128)(2,1)S(1)} collective-permute-done((bf16[512,512]{1,0:T(8,128)(2,1)S(1)}, bf16[512,512]{1,0:T(8,128)(2,1)S(1)}, u32[]{:S(2)}, u32[]{:S(2)}) %collective-permute-start) | collective-permute-done | bytes 524320 | tf_op jit(solution)/shard_map/ppermute | solution.py:149
  65.3 0.0 copy-start
  65.3 1.6 %copy-done = bf16[1,1024,1024]{2,1,0:T(8,128)(2,1)S(1)} copy-done((bf16[1,1024,1024]{2,1,0:T(8,128)(2,1)S(1)}, bf16[1,1024,1024]{2,1,0:T(8,128)(2,1)}, u32[]{:S(2)}) %copy-start) | copy-done | bytes 2097176
  66.9 0.0 copy-start.6
  66.9 1.6 %copy-done.6 = bf16[1,1024,1024]{2,1,0:T(8,128)(2,1)S(1)} copy-done((bf16[1,1024,1024]{2,1,0:T(8,128)(2,1)S(1)}, bf16[1,1024,1024]{2,1,0:T(8,128)(2,1)}, u32[]{:S(2)}) %copy-start.6) | copy-done | bytes 2097176
  68.5 0.0 copy-start.7
  68.5 1.6 %copy-done.7 = bf16[1,1024,1024]{2,1,0:T(8,128)(2,1)S(1)} copy-done((bf16[1,1024,1024]{2,1,0:T(8,128)(2,1)S(1)}, bf16[1,1024,1024]{2,1,0:T(8,128)(2,1)}, u32[]{:S(2)}) %copy-start.7) | copy-done | bytes 2097176
  70.1 3.0 %hidden_part.1 = (bf16[512,1024]{1,0:T(8,128)(2,1)S(1)}, bf16[512,512]{1,0:T(8,128)(2,1)S(1)}) custom-call(s32[1]{0:T(128)} %bitcast.2.tp_ref, bf16[512,512]{1,0:T(8,128)(2,1)S(1)} %bitcast.12, bf16[512,512]{1,0:T(8,128)(2,1)S(1)} %collective-permute-done.other_ref, bf16[1,1024,1024]{2,1,0:T(8,128)(2,1)S(1)} %copy-done.6, ...), custom_call_target="tpu_custom_call" | custom-call | flops 2684354560 | bytes 5242880 | tf_op jit(solution)/shard_map/hidden_part/pallas_call | solution.py:88
  73.0 0.5 collective-permute-start.1
  73.5 0.7 keep_part.1
  74.2 0.0 copy-start.3
  74.2 0.0 copy-start.4
  74.3 0.0 copy-start.5
  74.3 0.8 collective-permute-done.1
  75.1 0.1 fusion
  75.2 36.5 %all_to_all.11 = bf16[64,8,512]{2,1,0:T(8,128)(2,1)S(1)} all-to-all(bf16[64,8,512]{2,1,0:T(8,128)(2,1)S(1)} %fusion), channel_id=1, replica_groups=mesh['grp'=2,'ep'=64,'tp'=2] {'ep'}, dimensions={0} | all-to-all | bytes 1048576 | tf_op jit(solution)/shard_map/all_to_all | solution.py:150
  111.7 0.0 copy-done.3
  111.7 0.0 copy-done.4
  111.7 0.6 combine.1
  112.3 2.9 %collective-permute-start.2 = (f32[64,128]{1,0:T(8,128)S(1)}, f32[64,128]{1,0:T(8,128)S(1)}, u32[]{:S(2)}, u32[]{:S(2)}) collective-permute-start(f32[64,128]{1,0:T(8,128)S(1)} %get-tuple-element.12.square_ref), channel_id=1, source_target_pairs={{0,1},{1,0},{2,3},{3,2},{4,5},{5,4},{6,7},{7,6},{8,9},{9,8},{10,11... | collective-permute-start | bytes 98312 | tf_op jit(solution)/shard_map/ppermute | solution.py:149
  115.2 0.9 collective-permute-done.2.other_ref
  116.0 0.0 copy-done.5
  116.0 0.7 norm.1
Async XLA Ops:
  0.0 0.8 copy-start.1
  0.8 0.7 copy-start.2
  60.4 4.9 %collective-permute-start = (bf16[512,512]{1,0:T(8,128)(2,1)S(1)}, bf16[512,512]{1,0:T(8,128)(2,1)S(1)}, u32[]{:S(2)}, u32[]{:S(2)}) collective-permute-start(bf16[512,512]{1,0:T(8,128)(2,1)S(1)} %bitcast.11), channel_id=1, source_target_pairs={{0,1},{1,0},{2,3},{3,2},{4,5},{5,4},{6,7},{7,6},{8,9},{9,8},{10,11... | collective-permute-start | bytes 1572872 | tf_op jit(solution)/shard_map/ppermute | solution.py:149
  65.3 1.6 %copy-start = (bf16[1,1024,1024]{2,1,0:T(8,128)(2,1)S(1)}, bf16[1,1024,1024]{2,1,0:T(8,128)(2,1)}, u32[]{:S(2)}) copy-start(bf16[1,1024,1024]{2,1,0:T(8,128)(2,1)} %down_ref.3) | copy-start | bytes 6291460
  66.9 1.6 %copy-start.6 = (bf16[1,1024,1024]{2,1,0:T(8,128)(2,1)S(1)}, bf16[1,1024,1024]{2,1,0:T(8,128)(2,1)}, u32[]{:S(2)}) copy-start(bf16[1,1024,1024]{2,1,0:T(8,128)(2,1)} %gate_ref.1) | copy-start | bytes 6291460
  68.5 1.6 %copy-start.7 = (bf16[1,1024,1024]{2,1,0:T(8,128)(2,1)S(1)}, bf16[1,1024,1024]{2,1,0:T(8,128)(2,1)}, u32[]{:S(2)}) copy-start(bf16[1,1024,1024]{2,1,0:T(8,128)(2,1)} %up_ref.1) | copy-start | bytes 6291460
  73.0 2.0 %collective-permute-start.1 = (bf16[512,512]{1,0:T(8,128)(2,1)S(1)}, bf16[512,512]{1,0:T(8,128)(2,1)S(1)}, u32[]{:S(2)}, u32[]{:S(2)}) collective-permute-start(bf16[512,512]{1,0:T(8,128)(2,1)S(1)} %get-tuple-element.10), channel_id=1, source_target_pairs={{0,1},{1,0},{2,3},{3,2},{4,5},{5,4},{6,7},{7,6},{8,9},{9,8},{10,11... | collective-permute-start | bytes 1572872 | tf_op jit(solution)/shard_map/ppermute | solution.py:149
  74.2 37.5 %copy-start.3 = (s32[64,4]{0,1:T(4,128)S(1)}, s32[64,4]{0,1:T(4,128)}, u32[]{:S(2)}) copy-start(s32[64,4]{0,1:T(4,128)} %param.8) | copy-start | bytes 3076
  74.2 37.4 %copy-start.4 = (f32[64,4]{0,1:T(4,128)S(1)}, f32[64,4]{0,1:T(4,128)}, u32[]{:S(2)}) copy-start(f32[64,4]{0,1:T(4,128)} %param.9) | copy-start | bytes 3076
  74.3 41.8 %copy-start.5 = (f32[512]{0:T(512)S(1)}, f32[512]{0:T(512)}, u32[]{:S(2)}) copy-start(f32[512]{0:T(512)} %param.13) | copy-start | bytes 6148
  112.3 3.7 %collective-permute-start.2 = (f32[64,128]{1,0:T(8,128)S(1)}, f32[64,128]{1,0:T(8,128)S(1)}, u32[]{:S(2)}, u32[]{:S(2)}) collective-permute-start(f32[64,128]{1,0:T(8,128)S(1)} %get-tuple-element.12.square_ref), channel_id=1, source_target_pairs={{0,1},{1,0},{2,3},{3,2},{4,5},{5,4},{6,7},{7,6},{8,9},{9,8},{10,11... | collective-permute-start | bytes 98312 | tf_op jit(solution)/shard_map/ppermute | solution.py:149

commit v3 on v2

--- a/solution.py
+++ b/solution.py
@@ -11,6 +11,7 @@
 f32, bf16, i32 = jnp.float32, jnp.bfloat16, jnp.int32
 VMEM = pl.BlockSpec(memory_space=pltpu.VMEM)
 SMEM = pl.BlockSpec(memory_space=pltpu.SMEM)
+HBM = pl.BlockSpec(memory_space=pltpu.HBM)
 
 
 def call(body, name, mib, in_specs, out_shape, scratch=(), cost=None):
@@ -30,6 +31,10 @@
     return lax.dot_general(a, b, (dims, ((), ())), preferred_element_type=f32)
 
 
+def in_hbm(array):
+    return pltpu.with_memory_space_constraint(array, pltpu.HBM)
+
+
 def iota(shape, dim):
     return lax.broadcasted_iota(i32, shape, dim)
 
@@ -45,60 +50,101 @@
     return named, dot(named.astype(bf16), earlier.astype(bf16))
 
 
-def pack_body(ids_ref, hidden_ref, out_ref, *, expert_count, capacity):
-    named, rank = slot_ranks(ids_ref[...], expert_count)
-    code = jnp.where(named > 0, rank, -1.0).astype(bf16)
+def pack_body(ids_hbm, hidden_hbm, out_ref, ids_ref, hidden_ref, sems, *, expert_count, capacity):
+    ids_copy = pltpu.make_async_copy(ids_hbm, ids_ref, sems.at[0])
+    hidden_copy = pltpu.make_async_copy(hidden_hbm, hidden_ref, sems.at[1])
+    ids_copy.start()
+    hidden_copy.start()
     slots = expert_count * capacity
     spread = iota((slots, expert_count), 0) // capacity == iota((slots, expert_count), 1)
     spread = jnp.where(spread, 1.0, 0.0).astype(bf16)
+    ids_copy.wait()
+    named, rank = slot_ranks(ids_ref[...], expert_count)
+    code = jnp.where(named > 0, rank, -1.0).astype(bf16)
     wanted = dot(spread, code)
     own = (iota(wanted.shape, 0) % capacity).astype(f32)
     placing = jnp.where(wanted == own, 1.0, 0.0).astype(bf16)
+    hidden_copy.wait()
     out_ref[...] = dot(placing, hidden_ref[...]).astype(bf16)
 
 
 def pack(ids, hidden, expert_count, capacity):
     body = functools.partial(pack_body, expert_count=expert_count, capacity=capacity)
     out = jax.ShapeDtypeStruct((expert_count * capacity, hidden.shape[1]), bf16)
-    return call(body, "pack", 4, [VMEM] * 2, out)(ids, hidden)
-
-
-def hidden_body(tp_ref, own_ref, other_ref, gate_ref, up_ref, down_ref, act_ref, send_ref, *, tile):
+    scratch = [pltpu.VMEM(ids.shape, i32), pltpu.VMEM(hidden.shape, bf16), pltpu.SemaphoreType.DMA((2,))]
+    return call(body, "pack", 4, [HBM] * 2, out, scratch)(in_hbm(ids), in_hbm(hidden))
+
+
+def own_body(tp_ref, own_ref, gate_hbm, up_hbm, down_hbm, gate_out, up_out, gate_rest, up_rest, down_send, down_keep, gate_ref, up_ref, sems, *, tile):
     half = own_ref.shape[1]
-    units = gate_ref.shape[2]
-    mine = pl.multiple_of(tp_ref[0] * half, half)
-    theirs = pl.multiple_of((1 - tp_ref[0]) * half, half)
-    own, other = own_ref[...], other_ref[...]
-    for start in range(0, units, tile):
+    units = gate_ref.shape[1]
+    steps = units // tile
+    mine = pl.ds(pl.multiple_of(tp_ref[0] * half, half), half)
+    theirs = pl.ds(pl.multiple_of((1 - tp_ref[0]) * half, half), half)
+    copies = []
+    for j in range(steps):
+        at = slice(j * tile, (j + 1) * tile)
+        for source, target in ((gate_hbm, gate_ref), (up_hbm, up_ref)):
+            copies.append(pltpu.make_async_copy(source.at[0, mine, at], target.at[:, at], sems.at[len(copies)]))
+    for source, target in (
+        (gate_hbm.at[0, theirs, :], gate_rest),
+        (up_hbm.at[0, theirs, :], up_rest),
+        (down_hbm.at[0, :, theirs], down_send),
+        (down_hbm.at[0, :, mine], down_keep),
+    ):
+        copies.append(pltpu.make_async_copy(source, target, sems.at[len(copies)]))
+    for copy in copies:
+        copy.start()
+    own = own_ref[...]
+    for j in range(steps):
+        at = slice(j * tile, (j + 1) * tile)
+        copies[2 * j].wait()
+        gate_out[:, at] = dot(own, gate_ref[:, at])
+        copies[2 * j + 1].wait()
+        up_out[:, at] = dot(own, up_ref[:, at])
+    for copy in copies[2 * steps :]:
+        copy.wait()
+
+
+def own_part(tp, own, gate, up, down, tile=256):
+    rows, half = own.shape
+    units = gate.shape[2]
+    cost = pl.CostEstimate(flops=4 * rows * units * half, bytes_accessed=6 * units * units, transcendentals=0)
+    shape = jax.ShapeDtypeStruct
+    out = [shape((rows, units), f32)] * 2 + [shape((half, units), bf16)] * 2 + [shape((units, half), bf16)] * 2
+    scratch = [pltpu.VMEM((half, units), bf16)] * 2 + [pltpu.SemaphoreType.DMA((2 * (units // tile) + 4,))]
+    body = functools.partial(own_body, tile=tile)
+    return call(body, "own_part", 16, [SMEM, VMEM] + [HBM] * 3, out, scratch, cost)(tp, own, *map(in_hbm, (gate, up, down)))
+
+
+def hidden_body(other_ref, gate_in, up_in, gate_ref, up_ref, down_ref, act_ref, send_ref, *, tile):
+    other = other_ref[...]
+    for start in range(0, gate_ref.shape[1], tile):
         at = slice(start, start + tile)
-        gate = dot(own, gate_ref[0, pl.ds(mine, half), at]) + dot(other, gate_ref[0, pl.ds(theirs, half), at])
-        up = dot(own, up_ref[0, pl.ds(mine, half), at]) + dot(other, up_ref[0, pl.ds(theirs, half), at])
+        gate = gate_in[:, at] + dot(other, gate_ref[:, at])
+        up = up_in[:, at] + dot(other, up_ref[:, at])
         act_ref[:, at] = (gate / (1.0 + jnp.exp(-gate)) * up).astype(bf16)
-    send_ref[...] = dot(act_ref[...], down_ref[0, :, pl.ds(theirs, half)]).astype(bf16)
-
-
-def hidden_part(tp, own, other, gate, up, down, tile=256):
-    rows, half = own.shape
-    width, units = gate.shape[1:]
-    cost = pl.CostEstimate(
-        flops=2 * rows * units * (2 * width + half), bytes_accessed=2 * units * (2 * width + half), transcendentals=rows * units
-    )
+    send_ref[...] = dot(act_ref[...], down_ref[...]).astype(bf16)
+
+
+def hidden_part(other, gate_in, up_in, gate_rest, up_rest, down_send, tile=256):
+    rows, half = other.shape
+    units = gate_rest.shape[1]
+    cost = pl.CostEstimate(flops=6 * rows * units * half, bytes_accessed=6 * units * half, transcendentals=rows * units)
     out = [jax.ShapeDtypeStruct((rows, units), bf16), jax.ShapeDtypeStruct((rows, half), bf16)]
     body = functools.partial(hidden_body, tile=tile)
-    return call(body, "hidden_part", 16, [SMEM] + [VMEM] * 5, out, cost=cost)(tp, own, other, gate, up, down)
-
-
-def keep_body(tp_ref, act_ref, down_ref, out_ref):
-    half = out_ref.shape[1]
-    mine = pl.multiple_of(tp_ref[0] * half, half)
-    out_ref[...] = dot(act_ref[...], down_ref[0, :, pl.ds(mine, half)]).astype(bf16)
-
-
-def keep_part(tp, act, down, half):
+    return call(body, "hidden_part", 16, [VMEM] * 6, out, cost=cost)(other, gate_in, up_in, gate_rest, up_rest, down_send)
+
+
+def keep_body(act_ref, down_ref, out_ref):
+    out_ref[...] = dot(act_ref[...], down_ref[...]).astype(bf16)
+
+
+def keep_part(act, down_keep):
     rows, units = act.shape
+    half = down_keep.shape[1]
     cost = pl.CostEstimate(flops=2 * rows * units * half, bytes_accessed=2 * units * half, transcendentals=0)
-    out = jax.ShapeDtypeStruct((rows, half), bf16)
-    return call(keep_body, "keep_part", 8, [SMEM] + [VMEM] * 2, out, cost=cost)(tp, act, down)
+    return call(keep_body, "keep_part", 8, [VMEM] * 2, jax.ShapeDtypeStruct((rows, half), bf16), cost=cost)(act, down_keep)
 
 
 def combine_body(ids_ref, weight_ref, back_ref, out_ref, square_ref, *, expert_count, capacity):
@@ -151,9 +197,10 @@
         experts * capacity, half
     )
     own = exchange(pack(ids, hidden_state, experts, capacity))
-    act, send = hidden_part(tp, own, swap(own), gate_matrix, up_matrix, down_matrix)
+    gate_part, up_part, gate_rest, up_rest, down_send, down_keep = own_part(tp, own, gate_matrix, up_matrix, down_matrix)
+    act, send = hidden_part(swap(own), gate_part, up_part, gate_rest, up_rest, down_send)
     got = swap(send)
-    kept = keep_part(tp, act, down_matrix, half)
+    kept = keep_part(act, down_keep)
     answers = (kept.astype(f32) + got.astype(f32)).astype(bf16)
     combined, squares = combine(ids, weights, exchange(answers), experts, capacity)
     return norm(combined, squares, swap(squares), norm_gain, half * lax.axis_size("tp"))

time: 117 us -> 113 us (0.966)
  local copies, waits for them, and re-layouts: 6.31 us -> 0.02 us
  Pallas kernels: 5.54 us -> 9.8 us
  waiting for transfers between devices: 3.18 us -> 1.99 us
    unnamed x16 -> x6, local copies, waits for them, and re-layouts: 6.31 us -> 0.02 us
    pallas_call x3 -> x4, Pallas kernels: 4.2 us -> 8.46 us  [the longest x1 4.45 us: own_part(): call(body, 'own_part', 16, [SMEM, VMEM] + [HBM] * 3, out, scratch, cost)]
    ppermute x3, waiting for transfers between devices: 3.18 us -> 1.99 us  [shards(): swap = lambda a: lax.ppermute(a, 'tp', [(0, 1), (1, 0)])]
  transfers between devices with their start and end apart: 3 -> 3, of which waited for: 3 -> 2; matrix products, arithmetic and copies ran while one was open for 0% -> 0% of each run, Pallas kernels for 1% -> 5%
where the time goes in v3:
time: 113 us
  blocking collectives  95.2 us (84%)
  Pallas kernels  9.8 us (9%)
  starting transfers between devices  5.96 us (5%)
  waiting for transfers between devices  1.99 us (2%)
    all_to_all x2, blocking collectives, shards(): lax.all_to_all(a.reshape(experts, capacity, half), 'ep', 0, 0, tiled=True)  95.2 us
    ppermute x3, starting transfers between devices, shards(): swap = lambda a: lax.ppermute(a, 'tp', [(0, 1), (1, 0)])  5.96 us
    pallas_call x1, Pallas kernels, own_part(): call(body, 'own_part', 16, [SMEM, VMEM] + [HBM] * 3, out, scratch, cost)  4.45 us
  transfers between devices with their start and end apart: 3, of which 2 were waited for; matrix products, arithmetic and copies ran while one was open for 0% of the time, Pallas kernels for 5%

profile of v3, /device:TPU:33, one launch (start us, length us, event | category | flops | bytes accessed | tf_op | source)
XLA Modules:
  0.0 113.2 jit_solution(7277529555635171880)
XLA Ops:
  0.0 1.3 %pack.1 = bf16[512,512]{1,0:T(8,128)(2,1)S(1)} custom-call(s32[4,64]{1,0:T(4,128)} %bitcast.13, bf16[64,512]{1,0:T(8,128)(2,1)} %hidden_hbm.1), custom_call_target="tpu_custom_call" | custom-call | tf_op jit(solution)/shard_map/pack/pallas_call | solution.py:75
  1.3 58.4 %all_to_all.10 = bf16[64,8,512]{2,1,0:T(8,128)(2,1)S(1)} all-to-all(bf16[64,8,512]{2,1,0:T(8,128)(2,1)S(1)} %bitcast.10), channel_id=1, replica_groups=mesh['grp'=2,'ep'=64,'tp'=2] {'ep'}, dimensions={0} | all-to-all | bytes 1048576 | tf_op jit(solution)/shard_map/all_to_all | solution.py:196
  59.6 3.3 %collective-permute-start = (bf16[512,512]{1,0:T(8,128)(2,1)S(1)}, bf16[512,512]{1,0:T(8,128)(2,1)S(1)}, u32[]{:S(2)}, u32[]{:S(2)}) collective-permute-start(bf16[512,512]{1,0:T(8,128)(2,1)S(1)} %bitcast.11), channel_id=1, source_target_pairs={{0,1},{1,0},{2,3},{3,2},{4,5},{5,4},{6,7},{7,6},{8,9},{9,8},{10,11... | collective-permute-start | bytes 1572872 | tf_op jit(solution)/shard_map/ppermute | solution.py:195
  63.0 4.4 %own_part.1 = (f32[512,1024]{1,0:T(8,128)S(1)}, f32[512,1024]{1,0:T(8,128)S(1)}, bf16[512,1024]{1,0:T(8,128)(2,1)S(1)}, bf16[512,1024]{1,0:T(8,128)(2,1)S(1)}, b...) custom-call(s32[1]{0:T(128)} %bitcast.4.tp_ref, bf16[512,512]{1,0:T(8,128)(2,1)S(1)} %bitcast.12, ...), custom_call_target="tpu_custom_call" | custom-call | flops 1073741824 | bytes 6291456 | tf_op jit(solution)/shard_map/own_part/pallas_call | solution.py:117
  67.4 0.0 collective-permute-done.other_ref
  67.4 2.0 %hidden_part.1 = (bf16[512,1024]{1,0:T(8,128)(2,1)S(1)}, bf16[512,512]{1,0:T(8,128)(2,1)S(1)}) custom-call(bf16[512,512]{1,0:T(8,128)(2,1)S(1)} %collective-permute-done.other_ref, f32[512,1024]{1,0:T(8,128)S(1)} %get-tuple-element.15.gate_in, f32[512,1024]{1,0:T(8,128)S(1)} %get-tuple-element.16.up_in, bf16[512,1024]{1,0:T(8,128)(2,1)S(1)} %get-tuple-element.17.gate_ref, ...), custom_call_target="tpu_custom_call" | custom-call | flops 1610612736 | bytes 3145728 | tf_op jit(solution)/shard_map/hidden_part/pallas_call | solution.py:136
  69.5 0.1 collective-permute-start.1
  69.6 0.0 copy-start
  69.6 0.0 copy-start.1
  69.6 0.7 keep_part.1
  70.4 0.0 copy-start.2
  70.4 1.1 collective-permute-done.1
  71.5 0.1 fusion
  71.6 36.9 %all_to_all.11 = bf16[64,8,512]{2,1,0:T(8,128)(2,1)S(1)} all-to-all(bf16[64,8,512]{2,1,0:T(8,128)(2,1)S(1)} %fusion), channel_id=1, replica_groups=mesh['grp'=2,'ep'=64,'tp'=2] {'ep'}, dimensions={0} | all-to-all | bytes 1048576 | tf_op jit(solution)/shard_map/all_to_all | solution.py:196
  108.5 0.0 copy-done
  108.5 0.0 copy-done.1
  108.5 0.6 combine.1
  109.1 2.5 %collective-permute-start.2 = (f32[64,128]{1,0:T(8,128)S(1)}, f32[64,128]{1,0:T(8,128)S(1)}, u32[]{:S(2)}, u32[]{:S(2)}) collective-permute-start(f32[64,128]{1,0:T(8,128)S(1)} %get-tuple-element.24.square_ref), channel_id=1, source_target_pairs={{0,1},{1,0},{2,3},{3,2},{4,5},{5,4},{6,7},{7,6},{8,9},{9,8},{10,11... | collective-permute-start | bytes 98312 | tf_op jit(solution)/shard_map/ppermute | solution.py:195
  111.6 0.9 collective-permute-done.2.other_ref
  112.5 0.0 copy-done.2
  112.5 0.7 norm.1
Async XLA Ops:
  59.6 7.8 %collective-permute-start = (bf16[512,512]{1,0:T(8,128)(2,1)S(1)}, bf16[512,512]{1,0:T(8,128)(2,1)S(1)}, u32[]{:S(2)}, u32[]{:S(2)}) collective-permute-start(bf16[512,512]{1,0:T(8,128)(2,1)S(1)} %bitcast.11), channel_id=1, source_target_pairs={{0,1},{1,0},{2,3},{3,2},{4,5},{5,4},{6,7},{7,6},{8,9},{9,8},{10,11... | collective-permute-start | bytes 1572872 | tf_op jit(solution)/shard_map/ppermute | solution.py:195
  69.5 2.0 %collective-permute-start.1 = (bf16[512,512]{1,0:T(8,128)(2,1)S(1)}, bf16[512,512]{1,0:T(8,128)(2,1)S(1)}, u32[]{:S(2)}, u32[]{:S(2)}) collective-permute-start(bf16[512,512]{1,0:T(8,128)(2,1)S(1)} %get-tuple-element.22), channel_id=1, source_target_pairs={{0,1},{1,0},{2,3},{3,2},{4,5},{5,4},{6,7},{7,6},{8,9},{9,8},{10,11... | collective-permute-start | bytes 1572872 | tf_op jit(solution)/shard_map/ppermute | solution.py:195
  69.6 38.9 %copy-start = (s32[64,4]{0,1:T(4,128)S(1)}, s32[64,4]{0,1:T(4,128)}, u32[]{:S(2)}) copy-start(s32[64,4]{0,1:T(4,128)} %param.8) | copy-start | bytes 3076
  69.6 38.9 %copy-start.1 = (f32[64,4]{0,1:T(4,128)S(1)}, f32[64,4]{0,1:T(4,128)}, u32[]{:S(2)}) copy-start(f32[64,4]{0,1:T(4,128)} %param.9) | copy-start | bytes 3076
  70.4 42.1 %copy-start.2 = (f32[512]{0:T(512)S(1)}, f32[512]{0:T(512)}, u32[]{:S(2)}) copy-start(f32[512]{0:T(512)} %param.13) | copy-start | bytes 6148
  109.1 3.4 %collective-permute-start.2 = (f32[64,128]{1,0:T(8,128)S(1)}, f32[64,128]{1,0:T(8,128)S(1)}, u32[]{:S(2)}, u32[]{:S(2)}) collective-permute-start(f32[64,128]{1,0:T(8,128)S(1)} %get-tuple-element.24.square_ref), channel_id=1, source_target_pairs={{0,1},{1,0},{2,3},{3,2},{4,5},{5,4},{6,7},{7,6},{8,9},{9,8},{10,11... | collective-permute-start | bytes 98312 | tf_op jit(solution)/shard_map/ppermute | solution.py:195

commit v4 on v3

--- a/solution.py
+++ b/solution.py
@@ -12,6 +12,8 @@
 VMEM = pl.BlockSpec(memory_space=pltpu.VMEM)
 SMEM = pl.BlockSpec(memory_space=pltpu.SMEM)
 HBM = pl.BlockSpec(memory_space=pltpu.HBM)
+
+COVER = pl.CostEstimate(flops=1 << 34, bytes_accessed=1 << 16, transcendentals=0)
 
 
 def call(body, name, mib, in_specs, out_shape, scratch=(), cost=None):
@@ -72,68 +74,68 @@
     body = functools.partial(pack_body, expert_count=expert_count, capacity=capacity)
     out = jax.ShapeDtypeStruct((expert_count * capacity, hidden.shape[1]), bf16)
     scratch = [pltpu.VMEM(ids.shape, i32), pltpu.VMEM(hidden.shape, bf16), pltpu.SemaphoreType.DMA((2,))]
-    return call(body, "pack", 4, [HBM] * 2, out, scratch)(in_hbm(ids), in_hbm(hidden))
-
-
-def own_body(tp_ref, own_ref, gate_hbm, up_hbm, down_hbm, gate_out, up_out, gate_rest, up_rest, down_send, down_keep, gate_ref, up_ref, sems, *, tile):
+    return call(body, "pack", 4, [HBM] * 2, out, scratch, COVER)(in_hbm(ids), in_hbm(hidden))
+
+
+def own_body(tp_ref, own_ref, gate_ref, up_hbm, gate_out, up_out, up_rest, up_ref, sems, *, tile):
     half = own_ref.shape[1]
-    units = gate_ref.shape[1]
-    steps = units // tile
+    units = gate_out.shape[1]
     mine = pl.ds(pl.multiple_of(tp_ref[0] * half, half), half)
     theirs = pl.ds(pl.multiple_of((1 - tp_ref[0]) * half, half), half)
-    copies = []
-    for j in range(steps):
-        at = slice(j * tile, (j + 1) * tile)
-        for source, target in ((gate_hbm, gate_ref), (up_hbm, up_ref)):
-            copies.append(pltpu.make_async_copy(source.at[0, mine, at], target.at[:, at], sems.at[len(copies)]))
-    for source, target in (
-        (gate_hbm.at[0, theirs, :], gate_rest),
-        (up_hbm.at[0, theirs, :], up_rest),
-        (down_hbm.at[0, :, theirs], down_send),
-        (down_hbm.at[0, :, mine], down_keep),
-    ):
-        copies.append(pltpu.make_async_copy(source, target, sems.at[len(copies)]))
-    for copy in copies:
-        copy.start()
+    here = pltpu.make_async_copy(up_hbm.at[0, mine, :], up_ref, sems.at[0])
+    rest = pltpu.make_async_copy(up_hbm.at[0, theirs, :], up_rest, sems.at[1])
+    here.start()
+    rest.start()
     own = own_ref[...]
-    for j in range(steps):
-        at = slice(j * tile, (j + 1) * tile)
-        copies[2 * j].wait()
-        gate_out[:, at] = dot(own, gate_ref[:, at])
-        copies[2 * j + 1].wait()
+    tiles = [slice(start, start + tile) for start in range(0, units, tile)]
+    for at in tiles:
+        gate_out[:, at] = dot(own, gate_ref[0, mine, at])
+    here.wait()
+    for at in tiles:
         up_out[:, at] = dot(own, up_ref[:, at])
-    for copy in copies[2 * steps :]:
-        copy.wait()
-
-
-def own_part(tp, own, gate, up, down, tile=256):
+    rest.wait()
+
+
+def own_part(tp, own, gate, up, tile=256):
     rows, half = own.shape
     units = gate.shape[2]
-    cost = pl.CostEstimate(flops=4 * rows * units * half, bytes_accessed=6 * units * units, transcendentals=0)
-    shape = jax.ShapeDtypeStruct
-    out = [shape((rows, units), f32)] * 2 + [shape((half, units), bf16)] * 2 + [shape((units, half), bf16)] * 2
-    scratch = [pltpu.VMEM((half, units), bf16)] * 2 + [pltpu.SemaphoreType.DMA((2 * (units // tile) + 4,))]
+    cost = pl.CostEstimate(flops=4 * rows * units * half, bytes_accessed=4 * units * half, transcendentals=0)
+    out = [jax.ShapeDtypeStruct((rows, units), f32)] * 2 + [jax.ShapeDtypeStruct((half, units), bf16)]
+    scratch = [pltpu.VMEM((half, units), bf16), pltpu.SemaphoreType.DMA((2,))]
     body = functools.partial(own_body, tile=tile)
-    return call(body, "own_part", 16, [SMEM, VMEM] + [HBM] * 3, out, scratch, cost)(tp, own, *map(in_hbm, (gate, up, down)))
-
-
-def hidden_body(other_ref, gate_in, up_in, gate_ref, up_ref, down_ref, act_ref, send_ref, *, tile):
+    return call(body, "own_part", 8, [SMEM, VMEM, VMEM, HBM], out, scratch, cost)(tp, own, gate, in_hbm(up))
+
+
+def hidden_body(tp_ref, other_ref, gate_in, up_in, gate_ref, up_ref, down_hbm, act_ref, send_ref, down_keep, down_ref, sems, *, tile):
+    half = other_ref.shape[1]
+    mine = pl.ds(pl.multiple_of(tp_ref[0] * half, half), half)
+    theirs = pl.ds(pl.multiple_of((1 - tp_ref[0]) * half, half), half)
+    sent = pltpu.make_async_copy(down_hbm.at[0, :, theirs], down_ref, sems.at[0])
+    kept = pltpu.make_async_copy(down_hbm.at[0, :, mine], down_keep, sems.at[1])
+    sent.start()
+    kept.start()
     other = other_ref[...]
-    for start in range(0, gate_ref.shape[1], tile):
+    for start in range(0, gate_ref.shape[2], tile):
         at = slice(start, start + tile)
-        gate = gate_in[:, at] + dot(other, gate_ref[:, at])
+        gate = gate_in[:, at] + dot(other, gate_ref[0, theirs, at])
         up = up_in[:, at] + dot(other, up_ref[:, at])
         act_ref[:, at] = (gate / (1.0 + jnp.exp(-gate)) * up).astype(bf16)
+    sent.wait()
     send_ref[...] = dot(act_ref[...], down_ref[...]).astype(bf16)
-
-
-def hidden_part(other, gate_in, up_in, gate_rest, up_rest, down_send, tile=256):
+    kept.wait()
+
+
+def hidden_part(tp, other, gate_in, up_in, gate, up_rest, down, tile=256):
     rows, half = other.shape
-    units = gate_rest.shape[1]
+    units = gate.shape[2]
     cost = pl.CostEstimate(flops=6 * rows * units * half, bytes_accessed=6 * units * half, transcendentals=rows * units)
-    out = [jax.ShapeDtypeStruct((rows, units), bf16), jax.ShapeDtypeStruct((rows, half), bf16)]
+    shape = jax.ShapeDtypeStruct
+    out = [shape((rows, units), bf16), shape((rows, half), bf16), shape((units, half), bf16)]
+    scratch = [pltpu.VMEM((units, half), bf16), pltpu.SemaphoreType.DMA((2,))]
     body = functools.partial(hidden_body, tile=tile)
-    return call(body, "hidden_part", 16, [VMEM] * 6, out, cost=cost)(other, gate_in, up_in, gate_rest, up_rest, down_send)
+    return call(body, "hidden_part", 8, [SMEM] + [VMEM] * 5 + [HBM], out, scratch, cost)(
+        tp, other, gate_in, up_in, gate, up_rest, in_hbm(down)
+    )
 
 
 def keep_body(act_ref, down_ref, out_ref):
@@ -197,8 +199,8 @@
         experts * capacity, half
     )
     own = exchange(pack(ids, hidden_state, experts, capacity))
-    gate_part, up_part, gate_rest, up_rest, down_send, down_keep = own_part(tp, own, gate_matrix, up_matrix, down_matrix)
-    act, send = hidden_part(swap(own), gate_part, up_part, gate_rest, up_rest, down_send)
+    gate_part, up_part, up_rest = own_part(tp, own, gate_matrix, up_matrix)
+    act, send, down_keep = hidden_part(tp, swap(own), gate_part, up_part, gate_matrix, up_rest, down_matrix)
     got = swap(send)
     kept = keep_part(act, down_keep)
     answers = (kept.astype(f32) + got.astype(f32)).astype(bf16)

time: 113 us -> 113 us (level)
  transfers between devices with their start and end apart: 3 -> 3, of which waited for: 2 -> 2; matrix products, arithmetic and copies ran while one was open for 0% -> 0% of each run, Pallas kernels for 5% -> 3%
where the time goes in v4:
time: 113 us; the launch traced here: 112 us
  blocking collectives  95.2 us (84%)
  Pallas kernels  9.08 us (8%)
  starting transfers between devices  5.96 us (5%)
  waiting for transfers between devices  2 us (2%)
    all_to_all x2, blocking collectives, shards(): lax.all_to_all(a.reshape(experts, capacity, half), 'ep', 0, 0, tiled=True)  95.2 us
    ppermute x3, starting transfers between devices, shards(): swap = lambda a: lax.ppermute(a, 'tp', [(0, 1), (1, 0)])  5.96 us
    pallas_call x1, Pallas kernels, hidden_part(): call(body, 'hidden_part', 8, [SMEM] + [VMEM] * 5 + [HBM], out, scratch, c...  3.27 us
    pallas_call x1, Pallas kernels, own_part(): call(body, 'own_part', 8, [SMEM, VMEM, VMEM, HBM], out, scratch, cost)  2.34 us
  transfers between devices with their start and end apart: 3, of which 2 were waited for; matrix products, arithmetic and copies ran while one was open for 0% of the time, Pallas kernels for 3%

profile of v4, /device:TPU:33, one launch (start us, length us, event | category | flops | bytes accessed | tf_op | source)
XLA Modules:
  0.0 112.5 jit_solution(10931378214817301610)
XLA Ops:
  0.0 0.0 copy-start
  0.0 1.4 %pack.1 = bf16[512,512]{1,0:T(8,128)(2,1)S(1)} custom-call(s32[4,64]{1,0:T(4,128)} %bitcast.13, bf16[64,512]{1,0:T(8,128)(2,1)} %hidden_hbm.1), custom_call_target="tpu_custom_call" | custom-call | flops 17179869184 | bytes 65536 | tf_op jit(solution)/shard_map/pack/pallas_call | solution.py:77
  1.4 58.4 %all_to_all.10 = bf16[64,8,512]{2,1,0:T(8,128)(2,1)S(1)} all-to-all(bf16[64,8,512]{2,1,0:T(8,128)(2,1)S(1)} %bitcast.12), channel_id=1, replica_groups=mesh['grp'=2,'ep'=64,'tp'=2] {'ep'}, dimensions={0} | all-to-all | bytes 1048576 | tf_op jit(solution)/shard_map/all_to_all | solution.py:198
  59.8 3.3 %collective-permute-start = (bf16[512,512]{1,0:T(8,128)(2,1)S(1)}, bf16[512,512]{1,0:T(8,128)(2,1)S(1)}, u32[]{:S(2)}, u32[]{:S(2)}) collective-permute-start(bf16[512,512]{1,0:T(8,128)(2,1)S(1)} %bitcast.9), channel_id=1, source_target_pairs={{0,1},{1,0},{2,3},{3,2},{4,5},{5,4},{6,7},{7,6},{8,9},{9,8},{10,11... | collective-permute-start | bytes 1572872 | tf_op jit(solution)/shard_map/ppermute | solution.py:197
  63.1 0.0 copy-done
  63.1 2.3 %own_part.1 = (f32[512,1024]{1,0:T(8,128)S(1)}, f32[512,1024]{1,0:T(8,128)S(1)}, bf16[512,1024]{1,0:T(8,128)(2,1)S(1)}) custom-call(s32[1]{0:T(128)} %bitcast.2.tp_ref, bf16[512,512]{1,0:T(8,128)(2,1)S(1)} %bitcast.10, bf16[1,1024,1024]{2,1,0:T(8,128)(2,1)S(1)} %copy-done, bf16[1,1024,1024]{2,1,0:T(8,128)(2,1)} %up_hbm.1), custom_call_target="tpu_custom_call" | custom-call | flops 1073741824 | bytes 2097152 | tf_op jit(solution)/shard_map/own_part/pallas_call | solution.py:106
  65.5 0.0 collective-permute-done.other_ref
  65.5 3.3 %hidden_part.1 = (bf16[512,1024]{1,0:T(8,128)(2,1)S(1)}, bf16[512,512]{1,0:T(8,128)(2,1)S(1)}, bf16[1024,512]{1,0:T(8,128)(2,1)S(1)}) custom-call(s32[1]{0:T(128)} %bitcast.2.tp_ref, bf16[512,512]{1,0:T(8,128)(2,1)S(1)} %collective-permute-done.other_ref, f32[512,1024]{1,0:T(8,128)S(1)} %get-tuple-element.13.gate_in, ...), custom_call_target="tpu_custom_call" | custom-call | flops 1610612736 | bytes 3145728 | tf_op jit(solution)/shard_map/hidden_part/pallas_call | solution.py:136
  68.8 0.1 collective-permute-start.1
  68.9 0.0 copy-start.1
  68.9 0.0 copy-start.2
  68.9 0.7 keep_part.1
  69.6 0.0 copy-start.3
  69.6 1.1 %collective-permute-done.1 = bf16[512,512]{1,0:T(8,128)(2,1)S(1)} collective-permute-done((bf16[512,512]{1,0:T(8,128)(2,1)S(1)}, bf16[512,512]{1,0:T(8,128)(2,1)S(1)}, u32[]{:S(2)}, u32[]{:S(2)}) %collective-permute-start.1) | collective-permute-done | bytes 524320 | tf_op jit(solution)/shard_map/ppermute | solution.py:197
  70.8 0.1 fusion
  70.9 36.9 %all_to_all.11 = bf16[64,8,512]{2,1,0:T(8,128)(2,1)S(1)} all-to-all(bf16[64,8,512]{2,1,0:T(8,128)(2,1)S(1)} %fusion), channel_id=1, replica_groups=mesh['grp'=2,'ep'=64,'tp'=2] {'ep'}, dimensions={0} | all-to-all | bytes 1048576 | tf_op jit(solution)/shard_map/all_to_all | solution.py:198
  107.8 0.0 copy-done.1
  107.8 0.0 copy-done.2
  107.8 0.6 combine.1
  108.4 2.5 %collective-permute-start.2 = (f32[64,128]{1,0:T(8,128)S(1)}, f32[64,128]{1,0:T(8,128)S(1)}, u32[]{:S(2)}, u32[]{:S(2)}) collective-permute-start(f32[64,128]{1,0:T(8,128)S(1)} %get-tuple-element.20.square_ref), channel_id=1, source_target_pairs={{0,1},{1,0},{2,3},{3,2},{4,5},{5,4},{6,7},{7,6},{8,9},{9,8},{10,11... | collective-permute-start | bytes 98312 | tf_op jit(solution)/shard_map/ppermute | solution.py:197
  110.9 0.9 collective-permute-done.2.other_ref
  111.8 0.0 copy-done.3
  111.8 0.7 norm.1
Async XLA Ops:
  0.0 63.1 %copy-start = (bf16[1,1024,1024]{2,1,0:T(8,128)(2,1)S(1)}, bf16[1,1024,1024]{2,1,0:T(8,128)(2,1)}, u32[]{:S(2)}) copy-start(bf16[1,1024,1024]{2,1,0:T(8,128)(2,1)} %gate_ref.3) | copy-start | bytes 6291460
  59.8 5.7 %collective-permute-start = (bf16[512,512]{1,0:T(8,128)(2,1)S(1)}, bf16[512,512]{1,0:T(8,128)(2,1)S(1)}, u32[]{:S(2)}, u32[]{:S(2)}) collective-permute-start(bf16[512,512]{1,0:T(8,128)(2,1)S(1)} %bitcast.9), channel_id=1, source_target_pairs={{0,1},{1,0},{2,3},{3,2},{4,5},{5,4},{6,7},{7,6},{8,9},{9,8},{10,11... | collective-permute-start | bytes 1572872 | tf_op jit(solution)/shard_map/ppermute | solution.py:197
  68.8 2.0 %collective-permute-start.1 = (bf16[512,512]{1,0:T(8,128)(2,1)S(1)}, bf16[512,512]{1,0:T(8,128)(2,1)S(1)}, u32[]{:S(2)}, u32[]{:S(2)}) collective-permute-start(bf16[512,512]{1,0:T(8,128)(2,1)S(1)} %get-tuple-element.18), channel_id=1, source_target_pairs={{0,1},{1,0},{2,3},{3,2},{4,5},{5,4},{6,7},{7,6},{8,9},{9,8},{10,11... | collective-permute-start | bytes 1572872 | tf_op jit(solution)/shard_map/ppermute | solution.py:197
  68.9 38.9 %copy-start.1 = (s32[64,4]{0,1:T(4,128)S(1)}, s32[64,4]{0,1:T(4,128)}, u32[]{:S(2)}) copy-start(s32[64,4]{0,1:T(4,128)} %param.8) | copy-start | bytes 3076
  68.9 38.9 %copy-start.2 = (f32[64,4]{0,1:T(4,128)S(1)}, f32[64,4]{0,1:T(4,128)}, u32[]{:S(2)}) copy-start(f32[64,4]{0,1:T(4,128)} %param.9) | copy-start | bytes 3076
  69.6 42.1 %copy-start.3 = (f32[512]{0:T(512)S(1)}, f32[512]{0:T(512)}, u32[]{:S(2)}) copy-start(f32[512]{0:T(512)} %param.13) | copy-start | bytes 6148
  108.4 3.4 %collective-permute-start.2 = (f32[64,128]{1,0:T(8,128)S(1)}, f32[64,128]{1,0:T(8,128)S(1)}, u32[]{:S(2)}, u32[]{:S(2)}) collective-permute-start(f32[64,128]{1,0:T(8,128)S(1)} %get-tuple-element.20.square_ref), channel_id=1, source_target_pairs={{0,1},{1,0},{2,3},{3,2},{4,5},{5,4},{6,7},{7,6},{8,9},{9,8},{10,11... | collective-permute-start | bytes 98312 | tf_op jit(solution)/shard_map/ppermute | solution.py:197

commit v5 on v4

--- a/solution.py
+++ b/solution.py
@@ -77,42 +77,47 @@
     return call(body, "pack", 4, [HBM] * 2, out, scratch, COVER)(in_hbm(ids), in_hbm(hidden))
 
 
-def own_body(tp_ref, own_ref, gate_ref, up_hbm, gate_out, up_out, up_rest, up_ref, sems, *, tile):
+def own_body(tp_ref, own_ref, gate_ref, up_hbm, down_hbm, gate_out, up_out, up_rest, down_send, up_ref, sems, *, tile):
     half = own_ref.shape[1]
     units = gate_out.shape[1]
     mine = pl.ds(pl.multiple_of(tp_ref[0] * half, half), half)
     theirs = pl.ds(pl.multiple_of((1 - tp_ref[0]) * half, half), half)
     here = pltpu.make_async_copy(up_hbm.at[0, mine, :], up_ref, sems.at[0])
     rest = pltpu.make_async_copy(up_hbm.at[0, theirs, :], up_rest, sems.at[1])
+    down = pltpu.make_async_copy(down_hbm.at[0, :, theirs], down_send, sems.at[2])
     here.start()
-    rest.start()
     own = own_ref[...]
-    tiles = [slice(start, start + tile) for start in range(0, units, tile)]
-    for at in tiles:
+    for start in range(0, units, tile):
+        if start == tile:
+            rest.start()
+            down.start()
+        at = slice(start, start + tile)
         gate_out[:, at] = dot(own, gate_ref[0, mine, at])
     here.wait()
-    for at in tiles:
+    for start in range(0, units, tile):
+        at = slice(start, start + tile)
         up_out[:, at] = dot(own, up_ref[:, at])
     rest.wait()
-
-
-def own_part(tp, own, gate, up, tile=256):
+    down.wait()
+
+
+def own_part(tp, own, gate, up, down, tile=256):
     rows, half = own.shape
     units = gate.shape[2]
     cost = pl.CostEstimate(flops=4 * rows * units * half, bytes_accessed=4 * units * half, transcendentals=0)
-    out = [jax.ShapeDtypeStruct((rows, units), f32)] * 2 + [jax.ShapeDtypeStruct((half, units), bf16)]
-    scratch = [pltpu.VMEM((half, units), bf16), pltpu.SemaphoreType.DMA((2,))]
+    shape = jax.ShapeDtypeStruct
+    out = [shape((rows, units), f32)] * 2 + [shape((half, units), bf16), shape((units, half), bf16)]
+    scratch = [pltpu.VMEM((half, units), bf16), pltpu.SemaphoreType.DMA((3,))]
     body = functools.partial(own_body, tile=tile)
-    return call(body, "own_part", 8, [SMEM, VMEM, VMEM, HBM], out, scratch, cost)(tp, own, gate, in_hbm(up))
-
-
-def hidden_body(tp_ref, other_ref, gate_in, up_in, gate_ref, up_ref, down_hbm, act_ref, send_ref, down_keep, down_ref, sems, *, tile):
+    specs = [SMEM, VMEM, VMEM, HBM, HBM]
+    return call(body, "own_part", 8, specs, out, scratch, cost)(tp, own, gate, in_hbm(up), in_hbm(down))
+
+
+def hidden_body(tp_ref, other_ref, gate_in, up_in, gate_ref, up_ref, down_ref, down_hbm, act_ref, send_ref, down_keep, sems, *, tile):
     half = other_ref.shape[1]
     mine = pl.ds(pl.multiple_of(tp_ref[0] * half, half), half)
     theirs = pl.ds(pl.multiple_of((1 - tp_ref[0]) * half, half), half)
-    sent = pltpu.make_async_copy(down_hbm.at[0, :, theirs], down_ref, sems.at[0])
-    kept = pltpu.make_async_copy(down_hbm.at[0, :, mine], down_keep, sems.at[1])
-    sent.start()
+    kept = pltpu.make_async_copy(down_hbm.at[0, :, mine], down_keep, sems.at[0])
     kept.start()
     other = other_ref[...]
     for start in range(0, gate_ref.shape[2], tile):
@@ -120,21 +125,19 @@
         gate = gate_in[:, at] + dot(other, gate_ref[0, theirs, at])
         up = up_in[:, at] + dot(other, up_ref[:, at])
         act_ref[:, at] = (gate / (1.0 + jnp.exp(-gate)) * up).astype(bf16)
-    sent.wait()
     send_ref[...] = dot(act_ref[...], down_ref[...]).astype(bf16)
     kept.wait()
 
 
-def hidden_part(tp, other, gate_in, up_in, gate, up_rest, down, tile=256):
+def hidden_part(tp, other, gate_in, up_in, gate, up_rest, down_send, down, tile=256):
     rows, half = other.shape
     units = gate.shape[2]
     cost = pl.CostEstimate(flops=6 * rows * units * half, bytes_accessed=6 * units * half, transcendentals=rows * units)
     shape = jax.ShapeDtypeStruct
     out = [shape((rows, units), bf16), shape((rows, half), bf16), shape((units, half), bf16)]
-    scratch = [pltpu.VMEM((units, half), bf16), pltpu.SemaphoreType.DMA((2,))]
     body = functools.partial(hidden_body, tile=tile)
-    return call(body, "hidden_part", 8, [SMEM] + [VMEM] * 5 + [HBM], out, scratch, cost)(
-        tp, other, gate_in, up_in, gate, up_rest, in_hbm(down)
+    return call(body, "hidden_part", 8, [SMEM] + [VMEM] * 6 + [HBM], out, [pltpu.SemaphoreType.DMA((1,))], cost)(
+        tp, other, gate_in, up_in, gate, up_rest, down_send, in_hbm(down)
     )
 
 
@@ -149,7 +152,7 @@
     return call(keep_body, "keep_part", 8, [VMEM] * 2, jax.ShapeDtypeStruct((rows, half), bf16), cost=cost)(act, down_keep)
 
 
-def combine_body(ids_ref, weight_ref, back_ref, out_ref, square_ref, *, expert_count, capacity):
+def weigh_body(ids_ref, weight_ref, high_ref, low_ref, *, expert_count, capacity):
     ids = ids_ref[...]
     top, rows = ids.shape
     _, rank = slot_ranks(ids, expert_count)
@@ -161,19 +164,28 @@
         at = jnp.sum(jnp.where(row == experts, rank, 0.0), axis=0, keepdims=True).astype(i32)
         weights += jnp.where(row * capacity + at == places, weight_ref[k : k + 1], 0.0)
     high = weights.astype(bf16)
-    low = (weights - high.astype(f32)).astype(bf16)
+    high_ref[...] = high
+    low_ref[...] = (weights - high.astype(f32)).astype(bf16)
+
+
+def weigh(ids, weights, expert_count, capacity):
+    body = functools.partial(weigh_body, expert_count=expert_count, capacity=capacity)
+    out = [jax.ShapeDtypeStruct((expert_count * capacity, ids.shape[1]), bf16)] * 2
+    return call(body, "weigh", 4, [VMEM] * 2, out)(ids, weights)
+
+
+def combine_body(high_ref, low_ref, back_ref, out_ref, square_ref):
     back = back_ref[...]
     over = ((0,), (0,))
-    combined = dot(high, back, over) + dot(low, back, over)
+    combined = dot(high_ref[...], back, over) + dot(low_ref[...], back, over)
     out_ref[...] = combined
     square_ref[...] = jnp.broadcast_to(jnp.sum(combined * combined, axis=1, keepdims=True), square_ref.shape)
 
 
-def combine(ids, weights, back, expert_count, capacity):
-    rows = ids.shape[1]
-    body = functools.partial(combine_body, expert_count=expert_count, capacity=capacity)
+def combine(high, low, back):
+    rows = high.shape[1]
     out = [jax.ShapeDtypeStruct((rows, back.shape[1]), f32), jax.ShapeDtypeStruct((rows, 128), f32)]
-    return call(body, "combine", 4, [VMEM] * 3, out)(ids, weights, back)
+    return call(combine_body, "combine", 4, [VMEM] * 3, out)(high, low, back)
 
 
 def norm_body(combined_ref, square_ref, other_ref, gain_ref, out_ref, *, width):
@@ -199,12 +211,15 @@
         experts * capacity, half
     )
     own = exchange(pack(ids, hidden_state, experts, capacity))
-    gate_part, up_part, up_rest = own_part(tp, own, gate_matrix, up_matrix)
-    act, send, down_keep = hidden_part(tp, swap(own), gate_part, up_part, gate_matrix, up_rest, down_matrix)
+    gate_part, up_part, up_rest, down_send = own_part(tp, own, gate_matrix, up_matrix, down_matrix)
+    act, send, down_keep = hidden_part(
+        tp, swap(own), gate_part, up_part, gate_matrix, up_rest, down_send, down_matrix
+    )
     got = swap(send)
     kept = keep_part(act, down_keep)
+    kept, high, low = lax.optimization_barrier((kept, *weigh(ids, weights, experts, capacity)))
     answers = (kept.astype(f32) + got.astype(f32)).astype(bf16)
-    combined, squares = combine(ids, weights, exchange(answers), experts, capacity)
+    combined, squares = combine(high, low, exchange(answers))
     return norm(combined, squares, swap(squares), norm_gain, half * lax.axis_size("tp"))
 
 

time: 113 us -> 113 us (level)
    pallas_call x3 -> x4, Pallas kernels: 6.23 us -> 6.46 us  [the longest x1 3.09 us: hidden_part(): call(body, 'hidden_part', 8, [SMEM] + [VMEM] * 6 + [HBM], out, [pltpu.Sem...]
where the time goes in v5:
time: 113 us; the launch traced here: 112 us
  blocking collectives  95.2 us (84%)
  Pallas kernels  9.3 us (8%)
  starting transfers between devices  5.96 us (5%)
  waiting for transfers between devices  1.57 us (1%)
    all_to_all x2, blocking collectives, shards(): lax.all_to_all(a.reshape(experts, capacity, half), 'ep', 0, 0, tiled=True)  95.2 us
    ppermute x3, starting transfers between devices, shards(): swap = lambda a: lax.ppermute(a, 'tp', [(0, 1), (1, 0)])  5.96 us
    pallas_call x1, Pallas kernels, hidden_part(): call(body, 'hidden_part', 8, [SMEM] + [VMEM] * 6 + [HBM], out, [pltpu.Sem...  3.09 us
    pallas_call x1, Pallas kernels, own_part(): call(body, 'own_part', 8, specs, out, scratch, cost)  2.56 us
  transfers between devices with their start and end apart: 3, of which 2 were waited for; matrix products, arithmetic and copies ran while one was open for 0% of the time, Pallas kernels for 3%

profile of v5, /device:TPU:33, one launch (start us, length us, event | category | flops | bytes accessed | tf_op | source)
XLA Modules:
  0.0 112.3 jit_solution(13748199575322760178)
XLA Ops:
  0.0 0.0 copy-start
  0.0 1.4 %pack.1 = bf16[512,512]{1,0:T(8,128)(2,1)S(1)} custom-call(s32[4,64]{1,0:T(4,128)} %bitcast.14, bf16[64,512]{1,0:T(8,128)(2,1)} %hidden_hbm.1), custom_call_target="tpu_custom_call" | custom-call | flops 17179869184 | bytes 65536 | tf_op jit(solution)/shard_map/pack/pallas_call | solution.py:77
  1.4 58.4 %all_to_all.10 = bf16[64,8,512]{2,1,0:T(8,128)(2,1)S(1)} all-to-all(bf16[64,8,512]{2,1,0:T(8,128)(2,1)S(1)} %bitcast.12), channel_id=1, replica_groups=mesh['grp'=2,'ep'=64,'tp'=2] {'ep'}, dimensions={0} | all-to-all | bytes 1048576 | tf_op jit(solution)/shard_map/all_to_all | solution.py:210
  59.8 3.3 %collective-permute-start = (bf16[512,512]{1,0:T(8,128)(2,1)S(1)}, bf16[512,512]{1,0:T(8,128)(2,1)S(1)}, u32[]{:S(2)}, u32[]{:S(2)}) collective-permute-start(bf16[512,512]{1,0:T(8,128)(2,1)S(1)} %bitcast.10), channel_id=1, source_target_pairs={{0,1},{1,0},{2,3},{3,2},{4,5},{5,4},{6,7},{7,6},{8,9},{9,8},{10,11... | collective-permute-start | bytes 1572872 | tf_op jit(solution)/shard_map/ppermute | solution.py:209
  63.1 0.0 copy-done
  63.1 2.6 %own_part.1 = (f32[512,1024]{1,0:T(8,128)S(1)}, f32[512,1024]{1,0:T(8,128)S(1)}, bf16[512,1024]{1,0:T(8,128)(2,1)S(1)}, bf16[1024,512]{1,0:T(8,128)(2,1)S(1)}) custom-call(s32[1]{0:T(128)} %bitcast.tp_ref, bf16[512,512]{1,0:T(8,128)(2,1)S(1)} %bitcast.11, bf16[1,1024,1024]{2,1,0:T(8,128)(2,1)S(1)} %copy-done, bf16[1,1024,1024]{2,1,0:T(8,128)(2,1)} %up_hbm.1, ...), custom_call_target="tpu_custom_call" | custom-call | flops 1073741824 | bytes 2097152 | tf_op jit(solution)/shard_map/own_part/pallas_call | solution.py:113
  65.7 0.0 collective-permute-done.other_ref
  65.7 0.0 copy-start.2
  65.7 0.0 copy-start.3
  65.7 3.1 %hidden_part.1 = (bf16[512,1024]{1,0:T(8,128)(2,1)S(1)}, bf16[512,512]{1,0:T(8,128)(2,1)S(1)}, bf16[1024,512]{1,0:T(8,128)(2,1)S(1)}) custom-call(s32[1]{0:T(128)} %bitcast.tp_ref, bf16[512,512]{1,0:T(8,128)(2,1)S(1)} %collective-permute-done.other_ref, f32[512,1024]{1,0:T(8,128)S(1)} %get-tuple-element.19.gate_in, f32[512,1024]{1,0:T(8,128)S(1)} %get-tuple-element.20.up_in, ...), custom_call_target="tpu_custom_call" | custom-call | flops 1610612736 | bytes 3145728 | tf_op jit(solution)/shard_map/hidden_part/pallas_call | solution.py:139
  68.8 0.1 collective-permute-start.1
  69.0 0.0 copy-done.2
  69.0 0.0 copy-done.3
  69.0 0.4 weigh.1
  69.4 0.7 keep_part.1
  70.1 0.0 copy-start.1
  70.1 0.7 collective-permute-done.1
  70.8 0.1 fusion
  71.0 36.9 %all_to_all.11 = bf16[64,8,512]{2,1,0:T(8,128)(2,1)S(1)} all-to-all(bf16[64,8,512]{2,1,0:T(8,128)(2,1)S(1)} %fusion), channel_id=1, replica_groups=mesh['grp'=2,'ep'=64,'tp'=2] {'ep'}, dimensions={0} | all-to-all | bytes 1048576 | tf_op jit(solution)/shard_map/all_to_all | solution.py:210
  107.8 0.4 combine.1
  108.2 2.5 %collective-permute-start.2 = (f32[64,128]{1,0:T(8,128)S(1)}, f32[64,128]{1,0:T(8,128)S(1)}, u32[]{:S(2)}, u32[]{:S(2)}) collective-permute-start(f32[64,128]{1,0:T(8,128)S(1)} %get-tuple-element.32.square_ref), channel_id=1, source_target_pairs={{0,1},{1,0},{2,3},{3,2},{4,5},{5,4},{6,7},{7,6},{8,9},{9,8},{10,11... | collective-permute-start | bytes 98312 | tf_op jit(solution)/shard_map/ppermute | solution.py:209
  110.7 0.9 collective-permute-done.2.other_ref
  111.6 0.0 copy-done.1
  111.6 0.7 norm.1
Async XLA Ops:
  0.0 63.1 %copy-start = (bf16[1,1024,1024]{2,1,0:T(8,128)(2,1)S(1)}, bf16[1,1024,1024]{2,1,0:T(8,128)(2,1)}, u32[]{:S(2)}) copy-start(bf16[1,1024,1024]{2,1,0:T(8,128)(2,1)} %gate_ref.3) | copy-start | bytes 6291460
  59.8 5.9 %collective-permute-start = (bf16[512,512]{1,0:T(8,128)(2,1)S(1)}, bf16[512,512]{1,0:T(8,128)(2,1)S(1)}, u32[]{:S(2)}, u32[]{:S(2)}) collective-permute-start(bf16[512,512]{1,0:T(8,128)(2,1)S(1)} %bitcast.10), channel_id=1, source_target_pairs={{0,1},{1,0},{2,3},{3,2},{4,5},{5,4},{6,7},{7,6},{8,9},{9,8},{10,11... | collective-permute-start | bytes 1572872 | tf_op jit(solution)/shard_map/ppermute | solution.py:209
  65.7 3.3 %copy-start.2 = (s32[64,4]{0,1:T(4,128)S(1)}, s32[64,4]{0,1:T(4,128)}, u32[]{:S(2)}) copy-start(s32[64,4]{0,1:T(4,128)} %param.8) | copy-start | bytes 3076
  65.7 3.3 %copy-start.3 = (f32[64,4]{0,1:T(4,128)S(1)}, f32[64,4]{0,1:T(4,128)}, u32[]{:S(2)}) copy-start(f32[64,4]{0,1:T(4,128)} %param.9) | copy-start | bytes 3076
  68.8 2.0 %collective-permute-start.1 = (bf16[512,512]{1,0:T(8,128)(2,1)S(1)}, bf16[512,512]{1,0:T(8,128)(2,1)S(1)}, u32[]{:S(2)}, u32[]{:S(2)}) collective-permute-start(bf16[512,512]{1,0:T(8,128)(2,1)S(1)} %get-tuple-element.30), channel_id=1, source_target_pairs={{0,1},{1,0},{2,3},{3,2},{4,5},{5,4},{6,7},{7,6},{8,9},{9,8},{10,11... | collective-permute-start | bytes 1572872 | tf_op jit(solution)/shard_map/ppermute | solution.py:209
  70.1 41.5 %copy-start.1 = (f32[512]{0:T(512)S(1)}, f32[512]{0:T(512)}, u32[]{:S(2)}) copy-start(f32[512]{0:T(512)} %param.13) | copy-start | bytes 6148
  108.2 3.4 %collective-permute-start.2 = (f32[64,128]{1,0:T(8,128)S(1)}, f32[64,128]{1,0:T(8,128)S(1)}, u32[]{:S(2)}, u32[]{:S(2)}) collective-permute-start(f32[64,128]{1,0:T(8,128)S(1)} %get-tuple-element.32.square_ref), channel_id=1, source_target_pairs={{0,1},{1,0},{2,3},{3,2},{4,5},{5,4},{6,7},{7,6},{8,9},{9,8},{10,11... | collective-permute-start | bytes 98312 | tf_op jit(solution)/shard_map/ppermute | solution.py:209

commit v6 on v5

--- a/solution.py
+++ b/solution.py
@@ -113,12 +113,9 @@
     return call(body, "own_part", 8, specs, out, scratch, cost)(tp, own, gate, in_hbm(up), in_hbm(down))
 
 
-def hidden_body(tp_ref, other_ref, gate_in, up_in, gate_ref, up_ref, down_ref, down_hbm, act_ref, send_ref, down_keep, sems, *, tile):
+def hidden_body(tp_ref, other_ref, gate_in, up_in, gate_ref, up_ref, down_ref, act_ref, send_ref, *, tile):
     half = other_ref.shape[1]
-    mine = pl.ds(pl.multiple_of(tp_ref[0] * half, half), half)
     theirs = pl.ds(pl.multiple_of((1 - tp_ref[0]) * half, half), half)
-    kept = pltpu.make_async_copy(down_hbm.at[0, :, mine], down_keep, sems.at[0])
-    kept.start()
     other = other_ref[...]
     for start in range(0, gate_ref.shape[2], tile):
         at = slice(start, start + tile)
@@ -126,30 +123,30 @@
         up = up_in[:, at] + dot(other, up_ref[:, at])
         act_ref[:, at] = (gate / (1.0 + jnp.exp(-gate)) * up).astype(bf16)
     send_ref[...] = dot(act_ref[...], down_ref[...]).astype(bf16)
-    kept.wait()
-
-
-def hidden_part(tp, other, gate_in, up_in, gate, up_rest, down_send, down, tile=256):
+
+
+def hidden_part(tp, other, gate_in, up_in, gate, up_rest, down_send, tile=256):
     rows, half = other.shape
     units = gate.shape[2]
     cost = pl.CostEstimate(flops=6 * rows * units * half, bytes_accessed=6 * units * half, transcendentals=rows * units)
-    shape = jax.ShapeDtypeStruct
-    out = [shape((rows, units), bf16), shape((rows, half), bf16), shape((units, half), bf16)]
+    out = [jax.ShapeDtypeStruct((rows, units), bf16), jax.ShapeDtypeStruct((rows, half), bf16)]
     body = functools.partial(hidden_body, tile=tile)
-    return call(body, "hidden_part", 8, [SMEM] + [VMEM] * 6 + [HBM], out, [pltpu.SemaphoreType.DMA((1,))], cost)(
-        tp, other, gate_in, up_in, gate, up_rest, down_send, in_hbm(down)
-    )
-
-
-def keep_body(act_ref, down_ref, out_ref):
-    out_ref[...] = dot(act_ref[...], down_ref[...]).astype(bf16)
-
-
-def keep_part(act, down_keep):
+    return call(body, "hidden_part", 8, [SMEM] + [VMEM] * 6, out, cost=cost)(
+        tp, other, gate_in, up_in, gate, up_rest, down_send
+    )
+
+
+def keep_body(tp_ref, act_ref, down_ref, out_ref):
+    half = out_ref.shape[1]
+    mine = pl.ds(pl.multiple_of(tp_ref[0] * half, half), half)
+    out_ref[...] = dot(act_ref[...], down_ref[0, :, mine]).astype(bf16)
+
+
+def keep_part(tp, act, down, half):
     rows, units = act.shape
-    half = down_keep.shape[1]
     cost = pl.CostEstimate(flops=2 * rows * units * half, bytes_accessed=2 * units * half, transcendentals=0)
-    return call(keep_body, "keep_part", 8, [VMEM] * 2, jax.ShapeDtypeStruct((rows, half), bf16), cost=cost)(act, down_keep)
+    out = jax.ShapeDtypeStruct((rows, half), bf16)
+    return call(keep_body, "keep_part", 8, [SMEM] + [VMEM] * 2, out, cost=cost)(tp, act, down)
 
 
 def weigh_body(ids_ref, weight_ref, high_ref, low_ref, *, expert_count, capacity):
@@ -212,11 +209,9 @@
     )
     own = exchange(pack(ids, hidden_state, experts, capacity))
     gate_part, up_part, up_rest, down_send = own_part(tp, own, gate_matrix, up_matrix, down_matrix)
-    act, send, down_keep = hidden_part(
-        tp, swap(own), gate_part, up_part, gate_matrix, up_rest, down_send, down_matrix
-    )
+    act, send = hidden_part(tp, swap(own), gate_part, up_part, gate_matrix, up_rest, down_send)
     got = swap(send)
-    kept = keep_part(act, down_keep)
+    kept = keep_part(tp, act, down_matrix, half)
     kept, high, low = lax.optimization_barrier((kept, *weigh(ids, weights, experts, capacity)))
     answers = (kept.astype(f32) + got.astype(f32)).astype(bf16)
     combined, squares = combine(high, low, exchange(answers))

time: 113 us -> 111 us (0.982)
  no operation moved by 1% of the time
where the time goes in v6:
time: 111 us
  blocking collectives  95.2 us (86%)
  Pallas kernels  8.23 us (7%)
  starting transfers between devices  5.96 us (5%)
  waiting for transfers between devices  1.55 us (1%)
    all_to_all x2, blocking collectives, shards(): lax.all_to_all(a.reshape(experts, capacity, half), 'ep', 0, 0, tiled=True)  95.2 us
    ppermute x3, starting transfers between devices, shards(): swap = lambda a: lax.ppermute(a, 'tp', [(0, 1), (1, 0)])  5.96 us
    pallas_call x1, Pallas kernels, own_part(): call(body, 'own_part', 8, specs, out, scratch, cost)  2.56 us
  transfers between devices with their start and end apart: 3, of which 2 were waited for; matrix products, arithmetic and copies ran while one was open for 0% of the time, Pallas kernels for 3%

profile of v6, /device:TPU:33, one launch (start us, length us, event | category | flops | bytes accessed | tf_op | source)
XLA Modules:
  0.0 111.2 jit_solution(15563350267628707882)
XLA Ops:
  0.0 0.0 copy-start
  0.0 1.4 %pack.1 = bf16[512,512]{1,0:T(8,128)(2,1)S(1)} custom-call(s32[4,64]{1,0:T(4,128)} %bitcast.14, bf16[64,512]{1,0:T(8,128)(2,1)} %hidden_hbm.1), custom_call_target="tpu_custom_call" | custom-call | flops 17179869184 | bytes 65536 | tf_op jit(solution)/shard_map/pack/pallas_call | solution.py:77
  1.4 58.4 %all_to_all.10 = bf16[64,8,512]{2,1,0:T(8,128)(2,1)S(1)} all-to-all(bf16[64,8,512]{2,1,0:T(8,128)(2,1)S(1)} %bitcast.12), channel_id=1, replica_groups=mesh['grp'=2,'ep'=64,'tp'=2] {'ep'}, dimensions={0} | all-to-all | bytes 1048576 | tf_op jit(solution)/shard_map/all_to_all | solution.py:207
  59.8 3.3 %collective-permute-start = (bf16[512,512]{1,0:T(8,128)(2,1)S(1)}, bf16[512,512]{1,0:T(8,128)(2,1)S(1)}, u32[]{:S(2)}, u32[]{:S(2)}) collective-permute-start(bf16[512,512]{1,0:T(8,128)(2,1)S(1)} %bitcast.10), channel_id=1, source_target_pairs={{0,1},{1,0},{2,3},{3,2},{4,5},{5,4},{6,7},{7,6},{8,9},{9,8},{10,11... | collective-permute-start | bytes 1572872 | tf_op jit(solution)/shard_map/ppermute | solution.py:206
  63.1 0.0 copy-done
  63.1 2.6 %own_part.1 = (f32[512,1024]{1,0:T(8,128)S(1)}, f32[512,1024]{1,0:T(8,128)S(1)}, bf16[512,1024]{1,0:T(8,128)(2,1)S(1)}, bf16[1024,512]{1,0:T(8,128)(2,1)S(1)}) custom-call(s32[1]{0:T(128)} %bitcast.tp_ref, bf16[512,512]{1,0:T(8,128)(2,1)S(1)} %bitcast.11, bf16[1,1024,1024]{2,1,0:T(8,128)(2,1)S(1)} %copy-done, bf16[1,1024,1024]{2,1,0:T(8,128)(2,1)} %up_hbm.1, ...), custom_call_target="tpu_custom_call" | custom-call | flops 1073741824 | bytes 2097152 | tf_op jit(solution)/shard_map/own_part/pallas_call | solution.py:113
  65.7 0.0 collective-permute-done.other_ref
  65.7 0.0 copy-start.3
  65.7 0.0 copy-start.4
  65.7 0.0 copy-start.1
  65.7 2.0 %hidden_part.1 = (bf16[512,1024]{1,0:T(8,128)(2,1)S(1)}, bf16[512,512]{1,0:T(8,128)(2,1)S(1)}) custom-call(s32[1]{0:T(128)} %bitcast.tp_ref, bf16[512,512]{1,0:T(8,128)(2,1)S(1)} %collective-permute-done.other_ref, f32[512,1024]{1,0:T(8,128)S(1)} %get-tuple-element.18.gate_in, f32[512,1024]{1,0:T(8,128)S(1)} %get-tuple-element.19.up_in, ...), custom_call_target="tpu_custom_call" | custom-call | flops 1610612736 | bytes 3145728 | tf_op jit(solution)/shard_map/hidden_part/pallas_call | solution.py:134
  67.7 0.1 collective-permute-start.1
  67.9 0.0 copy-done.3
  67.9 0.0 copy-done.4
  67.9 0.4 weigh.1
  68.3 0.0 copy-done.1
  68.3 0.7 keep_part.1
  69.1 0.0 copy-start.2
  69.1 0.7 collective-permute-done.1
  69.8 0.1 fusion
  69.9 36.9 %all_to_all.11 = bf16[64,8,512]{2,1,0:T(8,128)(2,1)S(1)} all-to-all(bf16[64,8,512]{2,1,0:T(8,128)(2,1)S(1)} %fusion), channel_id=1, replica_groups=mesh['grp'=2,'ep'=64,'tp'=2] {'ep'}, dimensions={0} | all-to-all | bytes 1048576 | tf_op jit(solution)/shard_map/all_to_all | solution.py:207
  106.8 0.4 combine.1
  107.2 2.5 %collective-permute-start.2 = (f32[64,128]{1,0:T(8,128)S(1)}, f32[64,128]{1,0:T(8,128)S(1)}, u32[]{:S(2)}, u32[]{:S(2)}) collective-permute-start(f32[64,128]{1,0:T(8,128)S(1)} %get-tuple-element.30.square_ref), channel_id=1, source_target_pairs={{0,1},{1,0},{2,3},{3,2},{4,5},{5,4},{6,7},{7,6},{8,9},{9,8},{10,11... | collective-permute-start | bytes 98312 | tf_op jit(solution)/shard_map/ppermute | solution.py:206
  109.7 0.9 collective-permute-done.2.other_ref
  110.5 0.0 copy-done.2
  110.5 0.7 norm.1
Async XLA Ops:
  0.0 63.1 %copy-start = (bf16[1,1024,1024]{2,1,0:T(8,128)(2,1)S(1)}, bf16[1,1024,1024]{2,1,0:T(8,128)(2,1)}, u32[]{:S(2)}) copy-start(bf16[1,1024,1024]{2,1,0:T(8,128)(2,1)} %gate_ref.3) | copy-start | bytes 6291460
  59.8 5.9 %collective-permute-start = (bf16[512,512]{1,0:T(8,128)(2,1)S(1)}, bf16[512,512]{1,0:T(8,128)(2,1)S(1)}, u32[]{:S(2)}, u32[]{:S(2)}) collective-permute-start(bf16[512,512]{1,0:T(8,128)(2,1)S(1)} %bitcast.10), channel_id=1, source_target_pairs={{0,1},{1,0},{2,3},{3,2},{4,5},{5,4},{6,7},{7,6},{8,9},{9,8},{10,11... | collective-permute-start | bytes 1572872 | tf_op jit(solution)/shard_map/ppermute | solution.py:206
  65.7 2.2 %copy-start.3 = (s32[64,4]{0,1:T(4,128)S(1)}, s32[64,4]{0,1:T(4,128)}, u32[]{:S(2)}) copy-start(s32[64,4]{0,1:T(4,128)} %param.8) | copy-start | bytes 3076
  65.7 2.2 %copy-start.4 = (f32[64,4]{0,1:T(4,128)S(1)}, f32[64,4]{0,1:T(4,128)}, u32[]{:S(2)}) copy-start(f32[64,4]{0,1:T(4,128)} %param.9) | copy-start | bytes 3076
  65.7 2.6 %copy-start.1 = (bf16[1,1024,1024]{2,1,0:T(8,128)(2,1)S(1)}, bf16[1,1024,1024]{2,1,0:T(8,128)(2,1)}, u32[]{:S(2)}) copy-start(bf16[1,1024,1024]{2,1,0:T(8,128)(2,1)} %down_ref.1) | copy-start | bytes 6291460
  67.7 2.0 %collective-permute-start.1 = (bf16[512,512]{1,0:T(8,128)(2,1)S(1)}, bf16[512,512]{1,0:T(8,128)(2,1)S(1)}, u32[]{:S(2)}, u32[]{:S(2)}) collective-permute-start(bf16[512,512]{1,0:T(8,128)(2,1)S(1)} %get-tuple-element.28), channel_id=1, source_target_pairs={{0,1},{1,0},{2,3},{3,2},{4,5},{5,4},{6,7},{7,6},{8,9},{9,8},{10,11... | collective-permute-start | bytes 1572872 | tf_op jit(solution)/shard_map/ppermute | solution.py:206
  69.1 41.5 %copy-start.2 = (f32[512]{0:T(512)S(1)}, f32[512]{0:T(512)}, u32[]{:S(2)}) copy-start(f32[512]{0:T(512)} %param.13) | copy-start | bytes 6148
  107.2 3.4 %collective-permute-start.2 = (f32[64,128]{1,0:T(8,128)S(1)}, f32[64,128]{1,0:T(8,128)S(1)}, u32[]{:S(2)}, u32[]{:S(2)}) collective-permute-start(f32[64,128]{1,0:T(8,128)S(1)} %get-tuple-element.30.square_ref), channel_id=1, source_target_pairs={{0,1},{1,0},{2,3},{3,2},{4,5},{5,4},{6,7},{7,6},{8,9},{9,8},{10,11... | collective-permute-start | bytes 98312 | tf_op jit(solution)/shard_map/ppermute | solution.py:206

commit v7 on v6

--- a/solution.py
+++ b/solution.py
@@ -77,20 +77,17 @@
     return call(body, "pack", 4, [HBM] * 2, out, scratch, COVER)(in_hbm(ids), in_hbm(hidden))
 
 
-def own_body(tp_ref, own_ref, gate_ref, up_hbm, down_hbm, gate_out, up_out, up_rest, down_send, up_ref, sems, *, tile):
+def own_body(tp_ref, own_ref, gate_ref, up_hbm, gate_out, up_out, up_rest, up_ref, sems, *, tile):
     half = own_ref.shape[1]
     units = gate_out.shape[1]
     mine = pl.ds(pl.multiple_of(tp_ref[0] * half, half), half)
     theirs = pl.ds(pl.multiple_of((1 - tp_ref[0]) * half, half), half)
     here = pltpu.make_async_copy(up_hbm.at[0, mine, :], up_ref, sems.at[0])
     rest = pltpu.make_async_copy(up_hbm.at[0, theirs, :], up_rest, sems.at[1])
-    down = pltpu.make_async_copy(down_hbm.at[0, :, theirs], down_send, sems.at[2])
     here.start()
+    rest.start()
     own = own_ref[...]
     for start in range(0, units, tile):
-        if start == tile:
-            rest.start()
-            down.start()
         at = slice(start, start + tile)
         gate_out[:, at] = dot(own, gate_ref[0, mine, at])
     here.wait()
@@ -98,19 +95,16 @@
         at = slice(start, start + tile)
         up_out[:, at] = dot(own, up_ref[:, at])
     rest.wait()
-    down.wait()
-
-
-def own_part(tp, own, gate, up, down, tile=256):
+
+
+def own_part(tp, own, gate, up, tile=256):
     rows, half = own.shape
     units = gate.shape[2]
-    cost = pl.CostEstimate(flops=4 * rows * units * half, bytes_accessed=4 * units * half, transcendentals=0)
     shape = jax.ShapeDtypeStruct
-    out = [shape((rows, units), f32)] * 2 + [shape((half, units), bf16), shape((units, half), bf16)]
-    scratch = [pltpu.VMEM((half, units), bf16), pltpu.SemaphoreType.DMA((3,))]
+    out = [shape((rows, units), f32)] * 2 + [shape((half, units), bf16)]
+    scratch = [pltpu.VMEM((half, units), bf16), pltpu.SemaphoreType.DMA((2,))]
     body = functools.partial(own_body, tile=tile)
-    specs = [SMEM, VMEM, VMEM, HBM, HBM]
-    return call(body, "own_part", 8, specs, out, scratch, cost)(tp, own, gate, in_hbm(up), in_hbm(down))
+    return call(body, "own_part", 8, [SMEM, VMEM, VMEM, HBM], out, scratch)(tp, own, gate, in_hbm(up))
 
 
 def hidden_body(tp_ref, other_ref, gate_in, up_in, gate_ref, up_ref, down_ref, act_ref, send_ref, *, tile):
@@ -122,17 +116,17 @@
         gate = gate_in[:, at] + dot(other, gate_ref[0, theirs, at])
         up = up_in[:, at] + dot(other, up_ref[:, at])
         act_ref[:, at] = (gate / (1.0 + jnp.exp(-gate)) * up).astype(bf16)
-    send_ref[...] = dot(act_ref[...], down_ref[...]).astype(bf16)
-
-
-def hidden_part(tp, other, gate_in, up_in, gate, up_rest, down_send, tile=256):
+    send_ref[...] = dot(act_ref[...], down_ref[0, :, theirs]).astype(bf16)
+
+
+def hidden_part(tp, other, gate_in, up_in, gate, up_rest, down, tile=256):
     rows, half = other.shape
     units = gate.shape[2]
     cost = pl.CostEstimate(flops=6 * rows * units * half, bytes_accessed=6 * units * half, transcendentals=rows * units)
     out = [jax.ShapeDtypeStruct((rows, units), bf16), jax.ShapeDtypeStruct((rows, half), bf16)]
     body = functools.partial(hidden_body, tile=tile)
     return call(body, "hidden_part", 8, [SMEM] + [VMEM] * 6, out, cost=cost)(
-        tp, other, gate_in, up_in, gate, up_rest, down_send
+        tp, other, gate_in, up_in, gate, up_rest, down
     )
 
 
@@ -208,8 +202,8 @@
         experts * capacity, half
     )
     own = exchange(pack(ids, hidden_state, experts, capacity))
-    gate_part, up_part, up_rest, down_send = own_part(tp, own, gate_matrix, up_matrix, down_matrix)
-    act, send = hidden_part(tp, swap(own), gate_part, up_part, gate_matrix, up_rest, down_send)
+    gate_part, up_part, up_rest = own_part(tp, own, gate_matrix, up_matrix)
+    act, send = hidden_part(tp, swap(own), gate_part, up_part, gate_matrix, up_rest, down_matrix)
     got = swap(send)
     kept = keep_part(tp, act, down_matrix, half)
     kept, high, low = lax.optimization_barrier((kept, *weigh(ids, weights, experts, capacity)))

time: 111 us -> 111 us (level)
  no operation moved by 1% of the time
where the time goes in v7:
time: 111 us
  blocking collectives  95.2 us (86%)
  Pallas kernels  8.24 us (7%)
  starting transfers between devices  5.97 us (5%)
  waiting for transfers between devices  1.56 us (1%)
    all_to_all x2, blocking collectives, shards(): lax.all_to_all(a.reshape(experts, capacity, half), 'ep', 0, 0, tiled=True)  95.2 us
    ppermute x3, starting transfers between devices, shards(): swap = lambda a: lax.ppermute(a, 'tp', [(0, 1), (1, 0)])  5.97 us
    pallas_call x1, Pallas kernels, own_part(): call(body, 'own_part', 8, [SMEM, VMEM, VMEM, HBM], out, scratch)  2.53 us
  transfers between devices with their start and end apart: 3, of which 2 were waited for; matrix products, arithmetic and copies ran while one was open for 0% of the time, Pallas kernels for 3%

profile of v7, /device:TPU:33, one launch (start us, length us, event | category | flops | bytes accessed | tf_op | source)
XLA Modules:
  0.0 111.2 jit_solution(13835259786544685547)
XLA Ops:
  0.0 0.0 copy-start
  0.0 1.4 %pack.1 = bf16[512,512]{1,0:T(8,128)(2,1)S(1)} custom-call(s32[4,64]{1,0:T(4,128)} %bitcast.14, bf16[64,512]{1,0:T(8,128)(2,1)} %hidden_hbm.1), custom_call_target="tpu_custom_call" | custom-call | flops 17179869184 | bytes 65536 | tf_op jit(solution)/shard_map/pack/pallas_call | solution.py:77
  1.4 58.4 %all_to_all.10 = bf16[64,8,512]{2,1,0:T(8,128)(2,1)S(1)} all-to-all(bf16[64,8,512]{2,1,0:T(8,128)(2,1)S(1)} %bitcast.12), channel_id=1, replica_groups=mesh['grp'=2,'ep'=64,'tp'=2] {'ep'}, dimensions={0} | all-to-all | bytes 1048576 | tf_op jit(solution)/shard_map/all_to_all | solution.py:201
  59.8 3.3 %collective-permute-start = (bf16[512,512]{1,0:T(8,128)(2,1)S(1)}, bf16[512,512]{1,0:T(8,128)(2,1)S(1)}, u32[]{:S(2)}, u32[]{:S(2)}) collective-permute-start(bf16[512,512]{1,0:T(8,128)(2,1)S(1)} %bitcast.9), channel_id=1, source_target_pairs={{0,1},{1,0},{2,3},{3,2},{4,5},{5,4},{6,7},{7,6},{8,9},{9,8},{10,11... | collective-permute-start | bytes 1572872 | tf_op jit(solution)/shard_map/ppermute | solution.py:200
  63.1 0.0 copy-done
  63.1 0.0 copy-start.1
  63.1 2.5 %own_part.1 = (f32[512,1024]{1,0:T(8,128)S(1)}, f32[512,1024]{1,0:T(8,128)S(1)}, bf16[512,1024]{1,0:T(8,128)(2,1)S(1)}) custom-call(s32[1]{0:T(128)} %bitcast.tp_ref, bf16[512,512]{1,0:T(8,128)(2,1)S(1)} %bitcast.10, bf16[1,1024,1024]{2,1,0:T(8,128)(2,1)S(1)} %copy-done, bf16[1,1024,1024]{2,1,0:T(8,128)(2,1)} %up_hbm.1), custom_call_target="tpu_custom_call" | custom-call | tf_op jit(solution)/shard_map/own_part/pallas_call | solution.py:107
  65.7 0.0 collective-permute-done.other_ref
  65.7 0.0 copy-done.1
  65.7 0.0 copy-start.3
  65.7 0.0 copy-start.4
  65.7 2.0 %hidden_part.1 = (bf16[512,1024]{1,0:T(8,128)(2,1)S(1)}, bf16[512,512]{1,0:T(8,128)(2,1)S(1)}) custom-call(s32[1]{0:T(128)} %bitcast.tp_ref, bf16[512,512]{1,0:T(8,128)(2,1)S(1)} %collective-permute-done.other_ref, f32[512,1024]{1,0:T(8,128)S(1)} %get-tuple-element.17.gate_in, f32[512,1024]{1,0:T(8,128)S(1)} %get-tuple-element.18.up_in, ...), custom_call_target="tpu_custom_call" | custom-call | flops 1610612736 | bytes 3145728 | tf_op jit(solution)/shard_map/hidden_part/pallas_call | solution.py:128
  67.7 0.2 collective-permute-start.1
  67.9 0.0 copy-done.3
  67.9 0.0 copy-done.4
  67.9 0.4 weigh.1
  68.3 0.7 keep_part.1
  69.1 0.0 copy-start.2
  69.1 0.7 collective-permute-done.1
  69.8 0.1 fusion
  69.9 36.9 %all_to_all.11 = bf16[64,8,512]{2,1,0:T(8,128)(2,1)S(1)} all-to-all(bf16[64,8,512]{2,1,0:T(8,128)(2,1)S(1)} %fusion), channel_id=1, replica_groups=mesh['grp'=2,'ep'=64,'tp'=2] {'ep'}, dimensions={0} | all-to-all | bytes 1048576 | tf_op jit(solution)/shard_map/all_to_all | solution.py:201
  106.8 0.4 combine.1
  107.2 2.5 %collective-permute-start.2 = (f32[64,128]{1,0:T(8,128)S(1)}, f32[64,128]{1,0:T(8,128)S(1)}, u32[]{:S(2)}, u32[]{:S(2)}) collective-permute-start(f32[64,128]{1,0:T(8,128)S(1)} %get-tuple-element.28.square_ref), channel_id=1, source_target_pairs={{0,1},{1,0},{2,3},{3,2},{4,5},{5,4},{6,7},{7,6},{8,9},{9,8},{10,11... | collective-permute-start | bytes 98312 | tf_op jit(solution)/shard_map/ppermute | solution.py:200
  109.7 0.9 collective-permute-done.2.other_ref
  110.5 0.0 copy-done.2
  110.5 0.7 norm.1
Async XLA Ops:
  0.0 63.1 %copy-start = (bf16[1,1024,1024]{2,1,0:T(8,128)(2,1)S(1)}, bf16[1,1024,1024]{2,1,0:T(8,128)(2,1)}, u32[]{:S(2)}) copy-start(bf16[1,1024,1024]{2,1,0:T(8,128)(2,1)} %gate_ref.3) | copy-start | bytes 6291460
  59.8 5.9 %collective-permute-start = (bf16[512,512]{1,0:T(8,128)(2,1)S(1)}, bf16[512,512]{1,0:T(8,128)(2,1)S(1)}, u32[]{:S(2)}, u32[]{:S(2)}) collective-permute-start(bf16[512,512]{1,0:T(8,128)(2,1)S(1)} %bitcast.9), channel_id=1, source_target_pairs={{0,1},{1,0},{2,3},{3,2},{4,5},{5,4},{6,7},{7,6},{8,9},{9,8},{10,11... | collective-permute-start | bytes 1572872 | tf_op jit(solution)/shard_map/ppermute | solution.py:200
  63.1 2.6 %copy-start.1 = (bf16[1,1024,1024]{2,1,0:T(8,128)(2,1)S(1)}, bf16[1,1024,1024]{2,1,0:T(8,128)(2,1)}, u32[]{:S(2)}) copy-start(bf16[1,1024,1024]{2,1,0:T(8,128)(2,1)} %down_ref.3) | copy-start | bytes 6291460
  65.7 2.2 %copy-start.3 = (s32[64,4]{0,1:T(4,128)S(1)}, s32[64,4]{0,1:T(4,128)}, u32[]{:S(2)}) copy-start(s32[64,4]{0,1:T(4,128)} %param.8) | copy-start | bytes 3076
  65.7 2.2 %copy-start.4 = (f32[64,4]{0,1:T(4,128)S(1)}, f32[64,4]{0,1:T(4,128)}, u32[]{:S(2)}) copy-start(f32[64,4]{0,1:T(4,128)} %param.9) | copy-start | bytes 3076
  67.7 2.0 %collective-permute-start.1 = (bf16[512,512]{1,0:T(8,128)(2,1)S(1)}, bf16[512,512]{1,0:T(8,128)(2,1)S(1)}, u32[]{:S(2)}, u32[]{:S(2)}) collective-permute-start(bf16[512,512]{1,0:T(8,128)(2,1)S(1)} %get-tuple-element.26), channel_id=1, source_target_pairs={{0,1},{1,0},{2,3},{3,2},{4,5},{5,4},{6,7},{7,6},{8,9},{9,8},{10,11... | collective-permute-start | bytes 1572872 | tf_op jit(solution)/shard_map/ppermute | solution.py:200
  69.1 41.5 %copy-start.2 = (f32[512]{0:T(512)S(1)}, f32[512]{0:T(512)}, u32[]{:S(2)}) copy-start(f32[512]{0:T(512)} %param.13) | copy-start | bytes 6148
  107.2 3.4 %collective-permute-start.2 = (f32[64,128]{1,0:T(8,128)S(1)}, f32[64,128]{1,0:T(8,128)S(1)}, u32[]{:S(2)}, u32[]{:S(2)}) collective-permute-start(f32[64,128]{1,0:T(8,128)S(1)} %get-tuple-element.28.square_ref), channel_id=1, source_target_pairs={{0,1},{1,0},{2,3},{3,2},{4,5},{5,4},{6,7},{7,6},{8,9},{9,8},{10,11... | collective-permute-start | bytes 98312 | tf_op jit(solution)/shard_map/ppermute | solution.py:200

commit v8 on v6

--- a/solution.py
+++ b/solution.py
@@ -41,6 +41,10 @@
     return lax.broadcasted_iota(i32, shape, dim)
 
 
+def placed_from(ids, first, expert_count):
+    return jnp.where(ids >= first, ids - first, ids + (expert_count - first))
+
+
 def slot_ranks(ids, expert_count):
     top, rows = ids.shape
     experts = iota((expert_count, rows), 0)
@@ -52,7 +56,7 @@
     return named, dot(named.astype(bf16), earlier.astype(bf16))
 
 
-def pack_body(ids_hbm, hidden_hbm, out_ref, ids_ref, hidden_ref, sems, *, expert_count, capacity):
+def pack_body(ids_hbm, hidden_hbm, out_ref, ids_ref, hidden_ref, sems, *, first, expert_count, capacity):
     ids_copy = pltpu.make_async_copy(ids_hbm, ids_ref, sems.at[0])
     hidden_copy = pltpu.make_async_copy(hidden_hbm, hidden_ref, sems.at[1])
     ids_copy.start()
@@ -61,7 +65,7 @@
     spread = iota((slots, expert_count), 0) // capacity == iota((slots, expert_count), 1)
     spread = jnp.where(spread, 1.0, 0.0).astype(bf16)
     ids_copy.wait()
-    named, rank = slot_ranks(ids_ref[...], expert_count)
+    named, rank = slot_ranks(placed_from(ids_ref[...], first, expert_count), expert_count)
     code = jnp.where(named > 0, rank, -1.0).astype(bf16)
     wanted = dot(spread, code)
     own = (iota(wanted.shape, 0) % capacity).astype(f32)
@@ -70,8 +74,8 @@
     out_ref[...] = dot(placing, hidden_ref[...]).astype(bf16)
 
 
-def pack(ids, hidden, expert_count, capacity):
-    body = functools.partial(pack_body, expert_count=expert_count, capacity=capacity)
+def pack(ids, hidden, first, expert_count, capacity):
+    body = functools.partial(pack_body, first=first, expert_count=expert_count, capacity=capacity)
     out = jax.ShapeDtypeStruct((expert_count * capacity, hidden.shape[1]), bf16)
     scratch = [pltpu.VMEM(ids.shape, i32), pltpu.VMEM(hidden.shape, bf16), pltpu.SemaphoreType.DMA((2,))]
     return call(body, "pack", 4, [HBM] * 2, out, scratch, COVER)(in_hbm(ids), in_hbm(hidden))
@@ -149,8 +153,8 @@
     return call(keep_body, "keep_part", 8, [SMEM] + [VMEM] * 2, out, cost=cost)(tp, act, down)
 
 
-def weigh_body(ids_ref, weight_ref, high_ref, low_ref, *, expert_count, capacity):
-    ids = ids_ref[...]
+def weigh_body(ids_ref, weight_ref, high_ref, low_ref, *, first, expert_count, capacity):
+    ids = placed_from(ids_ref[...], first, expert_count)
     top, rows = ids.shape
     _, rank = slot_ranks(ids, expert_count)
     experts = iota((expert_count, rows), 0)
@@ -165,8 +169,8 @@
     low_ref[...] = (weights - high.astype(f32)).astype(bf16)
 
 
-def weigh(ids, weights, expert_count, capacity):
-    body = functools.partial(weigh_body, expert_count=expert_count, capacity=capacity)
+def weigh(ids, weights, first, expert_count, capacity):
+    body = functools.partial(weigh_body, first=first, expert_count=expert_count, capacity=capacity)
     out = [jax.ShapeDtypeStruct((expert_count * capacity, ids.shape[1]), bf16)] * 2
     return call(body, "weigh", 4, [VMEM] * 2, out)(ids, weights)
 
@@ -204,15 +208,17 @@
     tp = lax.axis_index("tp").reshape(1)
     ids, weights = expert_ids.T, route_weight.T
     swap = lambda a: lax.ppermute(a, "tp", [(0, 1), (1, 0)])
-    exchange = lambda a: lax.all_to_all(a.reshape(experts, capacity, half), "ep", 0, 0, tiled=True).reshape(
-        experts * capacity, half
-    )
-    own = exchange(pack(ids, hidden_state, experts, capacity))
+    first = experts - experts // 16
+    members = [[(first + place) % experts for place in range(experts)]]
+    exchange = lambda a: lax.all_to_all(
+        a.reshape(experts, capacity, half), "ep", 0, 0, tiled=True, axis_index_groups=members
+    ).reshape(experts * capacity, half)
+    own = exchange(pack(ids, hidden_state, first, experts, capacity))
     gate_part, up_part, up_rest, down_send = own_part(tp, own, gate_matrix, up_matrix, down_matrix)
     act, send = hidden_part(tp, swap(own), gate_part, up_part, gate_matrix, up_rest, down_send)
     got = swap(send)
     kept = keep_part(tp, act, down_matrix, half)
-    kept, high, low = lax.optimization_barrier((kept, *weigh(ids, weights, experts, capacity)))
+    kept, high, low = lax.optimization_barrier((kept, *weigh(ids, weights, first, experts, capacity)))
     answers = (kept.astype(f32) + got.astype(f32)).astype(bf16)
     combined, squares = combine(high, low, exchange(answers))
     return norm(combined, squares, swap(squares), norm_gain, half * lax.axis_size("tp"))

time: 111 us -> 106 us (0.955)
  blocking collectives: 95.2 us -> 88 us
  starting transfers between devices: 5.96 us -> 7.71 us
    all_to_all x2, blocking collectives: 95.2 us -> 88 us  [shards(): lax.all_to_all(a.reshape(experts, capacity, half), 'ep', 0, 0, tiled=True...]
    ppermute x3, starting transfers between devices: 5.96 us -> 7.71 us  [shards(): swap = lambda a: lax.ppermute(a, 'tp', [(0, 1), (1, 0)])]
where the time goes in v8:
time: 106 us
  blocking collectives  88 us (83%)
  Pallas kernels  8.23 us (8%)
  starting transfers between devices  7.71 us (7%)
  waiting for transfers between devices  1.55 us (1%)
    all_to_all x2, blocking collectives, shards(): lax.all_to_all(a.reshape(experts, capacity, half), 'ep', 0, 0, tiled=True...  88 us
    ppermute x3, starting transfers between devices, shards(): swap = lambda a: lax.ppermute(a, 'tp', [(0, 1), (1, 0)])  7.71 us
    pallas_call x1, Pallas kernels, own_part(): call(body, 'own_part', 8, specs, out, scratch, cost)  2.56 us
  transfers between devices with their start and end apart: 3, of which 2 were waited for; matrix products, arithmetic and copies ran while one was open for 0% of the time, Pallas kernels for 3%

profile of v8, /device:TPU:33, one launch (start us, length us, event | category | flops | bytes accessed | tf_op | source)
XLA Modules:
  0.0 105.8 jit_solution(9405357013772546820)
XLA Ops:
  0.0 0.0 copy-start
  0.0 1.4 %pack.1 = bf16[512,512]{1,0:T(8,128)(2,1)S(1)} custom-call(s32[4,64]{1,0:T(4,128)} %bitcast.14, bf16[64,512]{1,0:T(8,128)(2,1)} %hidden_hbm.1), custom_call_target="tpu_custom_call" | custom-call | flops 17179869184 | bytes 65536 | tf_op jit(solution)/shard_map/pack/pallas_call | solution.py:81
  1.4 52.5 %all_to_all.10 = bf16[64,8,512]{2,1,0:T(8,128)(2,1)S(1)} all-to-all(bf16[64,8,512]{2,1,0:T(8,128)(2,1)S(1)} %bitcast.12), channel_id=1, replica_groups={{120,122,124,126,0,2,4,6,8,10,12,14,16,18,20,22,24,26,28,30,32,34,36,38..., dimensions={0} | all-to-all | bytes 1048576 | tf_op jit(solution)/shard_map/all_to_all | solution.py:213
  53.9 3.8 %collective-permute-start = (bf16[512,512]{1,0:T(8,128)(2,1)S(1)}, bf16[512,512]{1,0:T(8,128)(2,1)S(1)}, u32[]{:S(2)}, u32[]{:S(2)}) collective-permute-start(bf16[512,512]{1,0:T(8,128)(2,1)S(1)} %bitcast.10), channel_id=1, source_target_pairs={{0,1},{1,0},{2,3},{3,2},{4,5},{5,4},{6,7},{7,6},{8,9},{9,8},{10,11... | collective-permute-start | bytes 1572872 | tf_op jit(solution)/shard_map/ppermute | solution.py:210
  57.7 0.0 copy-done
  57.7 2.6 %own_part.1 = (f32[512,1024]{1,0:T(8,128)S(1)}, f32[512,1024]{1,0:T(8,128)S(1)}, bf16[512,1024]{1,0:T(8,128)(2,1)S(1)}, bf16[1024,512]{1,0:T(8,128)(2,1)S(1)}) custom-call(s32[1]{0:T(128)} %bitcast.tp_ref, bf16[512,512]{1,0:T(8,128)(2,1)S(1)} %bitcast.11, bf16[1,1024,1024]{2,1,0:T(8,128)(2,1)S(1)} %copy-done, bf16[1,1024,1024]{2,1,0:T(8,128)(2,1)} %up_hbm.1, ...), custom_call_target="tpu_custom_call" | custom-call | flops 1073741824 | bytes 2097152 | tf_op jit(solution)/shard_map/own_part/pallas_call | solution.py:117
  60.3 0.0 collective-permute-done.other_ref
  60.3 0.0 copy-start.3
  60.3 0.0 copy-start.4
  60.3 0.0 copy-start.1
  60.4 2.0 %hidden_part.1 = (bf16[512,1024]{1,0:T(8,128)(2,1)S(1)}, bf16[512,512]{1,0:T(8,128)(2,1)S(1)}) custom-call(s32[1]{0:T(128)} %bitcast.tp_ref, bf16[512,512]{1,0:T(8,128)(2,1)S(1)} %collective-permute-done.other_ref, f32[512,1024]{1,0:T(8,128)S(1)} %get-tuple-element.18.gate_in, f32[512,1024]{1,0:T(8,128)S(1)} %get-tuple-element.19.up_in, ...), custom_call_target="tpu_custom_call" | custom-call | flops 1610612736 | bytes 3145728 | tf_op jit(solution)/shard_map/hidden_part/pallas_call | solution.py:138
  62.4 0.1 collective-permute-start.1
  62.5 0.0 copy-done.3
  62.5 0.0 copy-done.4
  62.5 0.4 weigh.1
  63.0 0.0 copy-done.1
  63.0 0.7 keep_part.1
  63.7 0.0 copy-start.2
  63.7 0.7 collective-permute-done.1
  64.4 0.1 fusion
  64.5 35.5 %all_to_all.11 = bf16[64,8,512]{2,1,0:T(8,128)(2,1)S(1)} all-to-all(bf16[64,8,512]{2,1,0:T(8,128)(2,1)S(1)} %fusion), channel_id=1, replica_groups={{120,122,124,126,0,2,4,6,8,10,12,14,16,18,20,22,24,26,28,30,32,34,36,38..., dimensions={0} | all-to-all | bytes 1048576 | tf_op jit(solution)/shard_map/all_to_all | solution.py:213
  100.0 0.4 combine.1
  100.4 3.8 %collective-permute-start.2 = (f32[64,128]{1,0:T(8,128)S(1)}, f32[64,128]{1,0:T(8,128)S(1)}, u32[]{:S(2)}, u32[]{:S(2)}) collective-permute-start(f32[64,128]{1,0:T(8,128)S(1)} %get-tuple-element.30.square_ref), channel_id=1, source_target_pairs={{0,1},{1,0},{2,3},{3,2},{4,5},{5,4},{6,7},{7,6},{8,9},{9,8},{10,11... | collective-permute-start | bytes 98312 | tf_op jit(solution)/shard_map/ppermute | solution.py:210
  104.2 0.9 collective-permute-done.2.other_ref
  105.1 0.0 copy-done.2
  105.1 0.7 norm.1
Async XLA Ops:
  0.0 57.7 %copy-start = (bf16[1,1024,1024]{2,1,0:T(8,128)(2,1)S(1)}, bf16[1,1024,1024]{2,1,0:T(8,128)(2,1)}, u32[]{:S(2)}) copy-start(bf16[1,1024,1024]{2,1,0:T(8,128)(2,1)} %gate_ref.3) | copy-start | bytes 6291460
  53.9 6.4 %collective-permute-start = (bf16[512,512]{1,0:T(8,128)(2,1)S(1)}, bf16[512,512]{1,0:T(8,128)(2,1)S(1)}, u32[]{:S(2)}, u32[]{:S(2)}) collective-permute-start(bf16[512,512]{1,0:T(8,128)(2,1)S(1)} %bitcast.10), channel_id=1, source_target_pairs={{0,1},{1,0},{2,3},{3,2},{4,5},{5,4},{6,7},{7,6},{8,9},{9,8},{10,11... | collective-permute-start | bytes 1572872 | tf_op jit(solution)/shard_map/ppermute | solution.py:210
  60.3 2.2 %copy-start.3 = (s32[64,4]{0,1:T(4,128)S(1)}, s32[64,4]{0,1:T(4,128)}, u32[]{:S(2)}) copy-start(s32[64,4]{0,1:T(4,128)} %param.8) | copy-start | bytes 3076
  60.3 2.2 %copy-start.4 = (f32[64,4]{0,1:T(4,128)S(1)}, f32[64,4]{0,1:T(4,128)}, u32[]{:S(2)}) copy-start(f32[64,4]{0,1:T(4,128)} %param.9) | copy-start | bytes 3076
  60.3 2.6 %copy-start.1 = (bf16[1,1024,1024]{2,1,0:T(8,128)(2,1)S(1)}, bf16[1,1024,1024]{2,1,0:T(8,128)(2,1)}, u32[]{:S(2)}) copy-start(bf16[1,1024,1024]{2,1,0:T(8,128)(2,1)} %down_ref.1) | copy-start | bytes 6291460
  62.4 2.0 %collective-permute-start.1 = (bf16[512,512]{1,0:T(8,128)(2,1)S(1)}, bf16[512,512]{1,0:T(8,128)(2,1)S(1)}, u32[]{:S(2)}, u32[]{:S(2)}) collective-permute-start(bf16[512,512]{1,0:T(8,128)(2,1)S(1)} %get-tuple-element.28), channel_id=1, source_target_pairs={{0,1},{1,0},{2,3},{3,2},{4,5},{5,4},{6,7},{7,6},{8,9},{9,8},{10,11... | collective-permute-start | bytes 1572872 | tf_op jit(solution)/shard_map/ppermute | solution.py:210
  63.7 41.4 %copy-start.2 = (f32[512]{0:T(512)S(1)}, f32[512]{0:T(512)}, u32[]{:S(2)}) copy-start(f32[512]{0:T(512)} %param.13) | copy-start | bytes 6148
  100.4 4.6 %collective-permute-start.2 = (f32[64,128]{1,0:T(8,128)S(1)}, f32[64,128]{1,0:T(8,128)S(1)}, u32[]{:S(2)}, u32[]{:S(2)}) collective-permute-start(f32[64,128]{1,0:T(8,128)S(1)} %get-tuple-element.30.square_ref), channel_id=1, source_target_pairs={{0,1},{1,0},{2,3},{3,2},{4,5},{5,4},{6,7},{7,6},{8,9},{9,8},{10,11... | collective-permute-start | bytes 98312 | tf_op jit(solution)/shard_map/ppermute | solution.py:210

commit v9 on v8

--- a/solution.py
+++ b/solution.py
@@ -153,6 +153,18 @@
     return call(keep_body, "keep_part", 8, [SMEM] + [VMEM] * 2, out, cost=cost)(tp, act, down)
 
 
+def add_body(kept_ref, got_ref, out_ref, *, turn):
+    rows = out_ref.shape[0]
+    for start, end, to in ((turn, rows, 0), (0, turn, rows - turn)):
+        total = kept_ref[start:end].astype(f32) + got_ref[start:end].astype(f32)
+        out_ref[to : to + end - start] = total.astype(bf16)
+
+
+def add_turned(kept, got, turn):
+    body = functools.partial(add_body, turn=turn)
+    return call(body, "add_turned", 4, [VMEM] * 2, jax.ShapeDtypeStruct(kept.shape, bf16))(kept, got)
+
+
 def weigh_body(ids_ref, weight_ref, high_ref, low_ref, *, first, expert_count, capacity):
     ids = placed_from(ids_ref[...], first, expert_count)
     top, rows = ids.shape
@@ -209,18 +221,23 @@
     ids, weights = expert_ids.T, route_weight.T
     swap = lambda a: lax.ppermute(a, "tp", [(0, 1), (1, 0)])
     first = experts - experts // 16
-    members = [[(first + place) % experts for place in range(experts)]]
-    exchange = lambda a: lax.all_to_all(
-        a.reshape(experts, capacity, half), "ep", 0, 0, tiled=True, axis_index_groups=members
+    back = experts - experts // 8
+    exchange = lambda a, first: lax.all_to_all(
+        a.reshape(experts, capacity, half),
+        "ep",
+        0,
+        0,
+        tiled=True,
+        axis_index_groups=[[(first + place) % experts for place in range(experts)]],
     ).reshape(experts * capacity, half)
-    own = exchange(pack(ids, hidden_state, first, experts, capacity))
+    own = exchange(pack(ids, hidden_state, first, experts, capacity), first)
     gate_part, up_part, up_rest, down_send = own_part(tp, own, gate_matrix, up_matrix, down_matrix)
     act, send = hidden_part(tp, swap(own), gate_part, up_part, gate_matrix, up_rest, down_send)
     got = swap(send)
     kept = keep_part(tp, act, down_matrix, half)
-    kept, high, low = lax.optimization_barrier((kept, *weigh(ids, weights, first, experts, capacity)))
-    answers = (kept.astype(f32) + got.astype(f32)).astype(bf16)
-    combined, squares = combine(high, low, exchange(answers))
+    kept, high, low = lax.optimization_barrier((kept, *weigh(ids, weights, back, experts, capacity)))
+    answers = add_turned(kept, got, (back - first) % experts * capacity)
+    combined, squares = combine(high, low, exchange(answers, back))
     return norm(combined, squares, swap(squares), norm_gain, half * lax.axis_size("tp"))
 
 

time: 106 us -> 107 us (level)
  no operation moved by 1% of the time
where the time goes in v9:
time: 107 us; the launch traced here: 106 us
  blocking collectives  87.9 us (82%)
  Pallas kernels  8.36 us (8%)
  starting transfers between devices  8.07 us (8%)
  waiting for transfers between devices  1.55 us (1%)
    all_to_all x2, blocking collectives, shards(): lax.all_to_all(a.reshape(experts, capacity, half), 'ep', 0, 0, tiled=True...  87.9 us
    ppermute x3, starting transfers between devices, shards(): swap = lambda a: lax.ppermute(a, 'tp', [(0, 1), (1, 0)])  8.07 us
    pallas_call x1, Pallas kernels, own_part(): call(body, 'own_part', 8, specs, out, scratch, cost)  2.56 us
  transfers between devices with their start and end apart: 3, of which 2 were waited for; matrix products, arithmetic and copies ran while one was open for 0% of the time, Pallas kernels for 3%

profile of v9, /device:TPU:33, one launch (start us, length us, event | category | flops | bytes accessed | tf_op | source)
XLA Modules:
  0.0 106.0 jit_solution(1383483310787612878)
XLA Ops:
  0.0 0.0 copy-start
  0.0 1.4 %pack.1 = bf16[512,512]{1,0:T(8,128)(2,1)S(1)} custom-call(s32[4,64]{1,0:T(4,128)} %bitcast.14, bf16[64,512]{1,0:T(8,128)(2,1)} %hidden_hbm.1), custom_call_target="tpu_custom_call" | custom-call | flops 17179869184 | bytes 65536 | tf_op jit(solution)/shard_map/pack/pallas_call | solution.py:81
  1.4 52.5 %all_to_all.10 = bf16[64,8,512]{2,1,0:T(8,128)(2,1)S(1)} all-to-all(bf16[64,8,512]{2,1,0:T(8,128)(2,1)S(1)} %bitcast.12), channel_id=1, replica_groups={{120,122,124,126,0,2,4,6,8,10,12,14,16,18,20,22,24,26,28,30,32,34,36,38..., dimensions={0} | all-to-all | bytes 1048576 | tf_op jit(solution)/shard_map/all_to_all | solution.py:225
  53.9 3.8 %collective-permute-start = (bf16[512,512]{1,0:T(8,128)(2,1)S(1)}, bf16[512,512]{1,0:T(8,128)(2,1)S(1)}, u32[]{:S(2)}, u32[]{:S(2)}) collective-permute-start(bf16[512,512]{1,0:T(8,128)(2,1)S(1)} %bitcast.10), channel_id=1, source_target_pairs={{0,1},{1,0},{2,3},{3,2},{4,5},{5,4},{6,7},{7,6},{8,9},{9,8},{10,11... | collective-permute-start | bytes 1572872 | tf_op jit(solution)/shard_map/ppermute | solution.py:222
  57.7 0.0 copy-done
  57.7 2.6 %own_part.1 = (f32[512,1024]{1,0:T(8,128)S(1)}, f32[512,1024]{1,0:T(8,128)S(1)}, bf16[512,1024]{1,0:T(8,128)(2,1)S(1)}, bf16[1024,512]{1,0:T(8,128)(2,1)S(1)}) custom-call(s32[1]{0:T(128)} %bitcast.tp_ref, bf16[512,512]{1,0:T(8,128)(2,1)S(1)} %bitcast.11, bf16[1,1024,1024]{2,1,0:T(8,128)(2,1)S(1)} %copy-done, bf16[1,1024,1024]{2,1,0:T(8,128)(2,1)} %up_hbm.1, ...), custom_call_target="tpu_custom_call" | custom-call | flops 1073741824 | bytes 2097152 | tf_op jit(solution)/shard_map/own_part/pallas_call | solution.py:117
  60.3 0.0 collective-permute-done.other_ref
  60.3 0.0 copy-start.3
  60.3 0.0 copy-start.4
  60.3 0.0 copy-start.1
  60.4 2.0 %hidden_part.1 = (bf16[512,1024]{1,0:T(8,128)(2,1)S(1)}, bf16[512,512]{1,0:T(8,128)(2,1)S(1)}) custom-call(s32[1]{0:T(128)} %bitcast.tp_ref, bf16[512,512]{1,0:T(8,128)(2,1)S(1)} %collective-permute-done.other_ref, f32[512,1024]{1,0:T(8,128)S(1)} %get-tuple-element.18.gate_in, f32[512,1024]{1,0:T(8,128)S(1)} %get-tuple-element.19.up_in, ...), custom_call_target="tpu_custom_call" | custom-call | flops 1610612736 | bytes 3145728 | tf_op jit(solution)/shard_map/hidden_part/pallas_call | solution.py:138
  62.4 0.1 collective-permute-start.1
  62.5 0.0 copy-done.3
  62.5 0.0 copy-done.4
  62.5 0.4 weigh.1
  63.0 0.0 copy-done.1
  63.0 0.7 keep_part.1.kept_ref
  63.7 0.0 copy-start.2
  63.7 0.7 collective-permute-done.1.got_ref
  64.4 0.1 add_turned.1
  64.5 35.4 %all_to_all.11 = bf16[64,8,512]{2,1,0:T(8,128)(2,1)S(1)} all-to-all(bf16[64,8,512]{2,1,0:T(8,128)(2,1)S(1)} %bitcast.8), channel_id=1, replica_groups={{112,114,116,118,120,122,124,126,0,2,4,6,8,10,12,14,16,18,20,22,24,26,2..., dimensions={0} | all-to-all | bytes 1048576 | tf_op jit(solution)/shard_map/all_to_all | solution.py:225
  99.9 0.4 combine.1
  100.3 4.1 %collective-permute-start.2 = (f32[64,128]{1,0:T(8,128)S(1)}, f32[64,128]{1,0:T(8,128)S(1)}, u32[]{:S(2)}, u32[]{:S(2)}) collective-permute-start(f32[64,128]{1,0:T(8,128)S(1)} %get-tuple-element.30.square_ref), channel_id=1, source_target_pairs={{0,1},{1,0},{2,3},{3,2},{4,5},{5,4},{6,7},{7,6},{8,9},{9,8},{10,11... | collective-permute-start | bytes 98312 | tf_op jit(solution)/shard_map/ppermute | solution.py:222
  104.4 0.9 collective-permute-done.2.other_ref
  105.3 0.0 copy-done.2
  105.3 0.7 norm.1
Async XLA Ops:
  0.0 57.7 %copy-start = (bf16[1,1024,1024]{2,1,0:T(8,128)(2,1)S(1)}, bf16[1,1024,1024]{2,1,0:T(8,128)(2,1)}, u32[]{:S(2)}) copy-start(bf16[1,1024,1024]{2,1,0:T(8,128)(2,1)} %gate_ref.3) | copy-start | bytes 6291460
  53.9 6.4 %collective-permute-start = (bf16[512,512]{1,0:T(8,128)(2,1)S(1)}, bf16[512,512]{1,0:T(8,128)(2,1)S(1)}, u32[]{:S(2)}, u32[]{:S(2)}) collective-permute-start(bf16[512,512]{1,0:T(8,128)(2,1)S(1)} %bitcast.10), channel_id=1, source_target_pairs={{0,1},{1,0},{2,3},{3,2},{4,5},{5,4},{6,7},{7,6},{8,9},{9,8},{10,11... | collective-permute-start | bytes 1572872 | tf_op jit(solution)/shard_map/ppermute | solution.py:222
  60.3 2.2 %copy-start.3 = (s32[64,4]{0,1:T(4,128)S(1)}, s32[64,4]{0,1:T(4,128)}, u32[]{:S(2)}) copy-start(s32[64,4]{0,1:T(4,128)} %param.8) | copy-start | bytes 3076
  60.3 2.2 %copy-start.4 = (f32[64,4]{0,1:T(4,128)S(1)}, f32[64,4]{0,1:T(4,128)}, u32[]{:S(2)}) copy-start(f32[64,4]{0,1:T(4,128)} %param.9) | copy-start | bytes 3076
  60.3 2.6 %copy-start.1 = (bf16[1,1024,1024]{2,1,0:T(8,128)(2,1)S(1)}, bf16[1,1024,1024]{2,1,0:T(8,128)(2,1)}, u32[]{:S(2)}) copy-start(bf16[1,1024,1024]{2,1,0:T(8,128)(2,1)} %down_ref.1) | copy-start | bytes 6291460
  62.4 2.0 %collective-permute-start.1 = (bf16[512,512]{1,0:T(8,128)(2,1)S(1)}, bf16[512,512]{1,0:T(8,128)(2,1)S(1)}, u32[]{:S(2)}, u32[]{:S(2)}) collective-permute-start(bf16[512,512]{1,0:T(8,128)(2,1)S(1)} %get-tuple-element.28), channel_id=1, source_target_pairs={{0,1},{1,0},{2,3},{3,2},{4,5},{5,4},{6,7},{7,6},{8,9},{9,8},{10,11... | collective-permute-start | bytes 1572872 | tf_op jit(solution)/shard_map/ppermute | solution.py:222
  63.7 41.6 %copy-start.2 = (f32[512]{0:T(512)S(1)}, f32[512]{0:T(512)}, u32[]{:S(2)}) copy-start(f32[512]{0:T(512)} %param.13) | copy-start | bytes 6148
  100.3 5.0 %collective-permute-start.2 = (f32[64,128]{1,0:T(8,128)S(1)}, f32[64,128]{1,0:T(8,128)S(1)}, u32[]{:S(2)}, u32[]{:S(2)}) collective-permute-start(f32[64,128]{1,0:T(8,128)S(1)} %get-tuple-element.30.square_ref), channel_id=1, source_target_pairs={{0,1},{1,0},{2,3},{3,2},{4,5},{5,4},{6,7},{7,6},{8,9},{9,8},{10,11... | collective-permute-start | bytes 98312 | tf_op jit(solution)/shard_map/ppermute | solution.py:222

commit v10 on v8

--- a/solution.py
+++ b/solution.py
@@ -153,7 +153,7 @@
     return call(keep_body, "keep_part", 8, [SMEM] + [VMEM] * 2, out, cost=cost)(tp, act, down)
 
 
-def weigh_body(ids_ref, weight_ref, high_ref, low_ref, *, first, expert_count, capacity):
+def weigh_body(ids_ref, weight_ref, out_ref, *, first, expert_count, capacity):
     ids = placed_from(ids_ref[...], first, expert_count)
     top, rows = ids.shape
     _, rank = slot_ranks(ids, expert_count)
@@ -165,28 +165,28 @@
         at = jnp.sum(jnp.where(row == experts, rank, 0.0), axis=0, keepdims=True).astype(i32)
         weights += jnp.where(row * capacity + at == places, weight_ref[k : k + 1], 0.0)
     high = weights.astype(bf16)
-    high_ref[...] = high
-    low_ref[...] = (weights - high.astype(f32)).astype(bf16)
+    out_ref[:, :rows] = high
+    out_ref[:, rows:] = (weights - high.astype(f32)).astype(bf16)
 
 
 def weigh(ids, weights, first, expert_count, capacity):
     body = functools.partial(weigh_body, first=first, expert_count=expert_count, capacity=capacity)
-    out = [jax.ShapeDtypeStruct((expert_count * capacity, ids.shape[1]), bf16)] * 2
+    out = jax.ShapeDtypeStruct((expert_count * capacity, 2 * ids.shape[1]), bf16)
     return call(body, "weigh", 4, [VMEM] * 2, out)(ids, weights)
 
 
-def combine_body(high_ref, low_ref, back_ref, out_ref, square_ref):
-    back = back_ref[...]
-    over = ((0,), (0,))
-    combined = dot(high_ref[...], back, over) + dot(low_ref[...], back, over)
+def combine_body(terms_ref, back_ref, out_ref, square_ref):
+    both = dot(terms_ref[...], back_ref[...], ((0,), (0,)))
+    rows = out_ref.shape[0]
+    combined = both[:rows] + both[rows:]
     out_ref[...] = combined
     square_ref[...] = jnp.broadcast_to(jnp.sum(combined * combined, axis=1, keepdims=True), square_ref.shape)
 
 
-def combine(high, low, back):
-    rows = high.shape[1]
+def combine(terms, back):
+    rows = terms.shape[1] // 2
     out = [jax.ShapeDtypeStruct((rows, back.shape[1]), f32), jax.ShapeDtypeStruct((rows, 128), f32)]
-    return call(combine_body, "combine", 4, [VMEM] * 3, out)(high, low, back)
+    return call(combine_body, "combine", 4, [VMEM] * 2, out)(terms, back)
 
 
 def norm_body(combined_ref, square_ref, other_ref, gain_ref, out_ref, *, width):
@@ -218,9 +218,9 @@
     act, send = hidden_part(tp, swap(own), gate_part, up_part, gate_matrix, up_rest, down_send)
     got = swap(send)
     kept = keep_part(tp, act, down_matrix, half)
-    kept, high, low = lax.optimization_barrier((kept, *weigh(ids, weights, first, experts, capacity)))
+    kept, terms = lax.optimization_barrier((kept, weigh(ids, weights, first, experts, capacity)))
     answers = (kept.astype(f32) + got.astype(f32)).astype(bf16)
-    combined, squares = combine(high, low, exchange(answers))
+    combined, squares = combine(terms, exchange(answers))
     return norm(combined, squares, swap(squares), norm_gain, half * lax.axis_size("tp"))
 
 

time: 106 us -> 106 us (level)
  no operation moved by 1% of the time
where the time goes in v10:
time: 106 us
  blocking collectives  88 us (83%)
  Pallas kernels  8.08 us (8%)
  starting transfers between devices  7.71 us (7%)
  waiting for transfers between devices  1.64 us (2%)
    all_to_all x2, blocking collectives, shards(): lax.all_to_all(a.reshape(experts, capacity, half), 'ep', 0, 0, tiled=True...  88 us
    ppermute x3, starting transfers between devices, shards(): swap = lambda a: lax.ppermute(a, 'tp', [(0, 1), (1, 0)])  7.71 us
    pallas_call x1, Pallas kernels, own_part(): call(body, 'own_part', 8, specs, out, scratch, cost)  2.56 us
  transfers between devices with their start and end apart: 3, of which 2 were waited for; matrix products, arithmetic and copies ran while one was open for 0% of the time, Pallas kernels for 3%

profile of v10, /device:TPU:33, one launch (start us, length us, event | category | flops | bytes accessed | tf_op | source)
XLA Modules:
  0.0 105.7 jit_solution(11695653623434086482)
XLA Ops:
  0.0 0.0 copy-start
  0.0 1.4 %pack.1 = bf16[512,512]{1,0:T(8,128)(2,1)S(1)} custom-call(s32[4,64]{1,0:T(4,128)} %bitcast.13, bf16[64,512]{1,0:T(8,128)(2,1)} %hidden_hbm.1), custom_call_target="tpu_custom_call" | custom-call | flops 17179869184 | bytes 65536 | tf_op jit(solution)/shard_map/pack/pallas_call | solution.py:81
  1.4 52.5 %all_to_all.10 = bf16[64,8,512]{2,1,0:T(8,128)(2,1)S(1)} all-to-all(bf16[64,8,512]{2,1,0:T(8,128)(2,1)S(1)} %bitcast.12), channel_id=1, replica_groups={{120,122,124,126,0,2,4,6,8,10,12,14,16,18,20,22,24,26,28,30,32,34,36,38..., dimensions={0} | all-to-all | bytes 1048576 | tf_op jit(solution)/shard_map/all_to_all | solution.py:213
  53.9 3.8 %collective-permute-start = (bf16[512,512]{1,0:T(8,128)(2,1)S(1)}, bf16[512,512]{1,0:T(8,128)(2,1)S(1)}, u32[]{:S(2)}, u32[]{:S(2)}) collective-permute-start(bf16[512,512]{1,0:T(8,128)(2,1)S(1)} %bitcast.10), channel_id=1, source_target_pairs={{0,1},{1,0},{2,3},{3,2},{4,5},{5,4},{6,7},{7,6},{8,9},{9,8},{10,11... | collective-permute-start | bytes 1572872 | tf_op jit(solution)/shard_map/ppermute | solution.py:210
  57.7 0.0 copy-done
  57.7 2.6 %own_part.1 = (f32[512,1024]{1,0:T(8,128)S(1)}, f32[512,1024]{1,0:T(8,128)S(1)}, bf16[512,1024]{1,0:T(8,128)(2,1)S(1)}, bf16[1024,512]{1,0:T(8,128)(2,1)S(1)}) custom-call(s32[1]{0:T(128)} %bitcast.tp_ref, bf16[512,512]{1,0:T(8,128)(2,1)S(1)} %bitcast.11, bf16[1,1024,1024]{2,1,0:T(8,128)(2,1)S(1)} %copy-done, bf16[1,1024,1024]{2,1,0:T(8,128)(2,1)} %up_hbm.1, ...), custom_call_target="tpu_custom_call" | custom-call | flops 1073741824 | bytes 2097152 | tf_op jit(solution)/shard_map/own_part/pallas_call | solution.py:117
  60.3 0.0 collective-permute-done.other_ref
  60.3 0.0 copy-start.2
  60.3 0.0 copy-start.3
  60.3 0.0 copy-start.1
  60.4 2.0 %hidden_part.1 = (bf16[512,1024]{1,0:T(8,128)(2,1)S(1)}, bf16[512,512]{1,0:T(8,128)(2,1)S(1)}) custom-call(s32[1]{0:T(128)} %bitcast.tp_ref, bf16[512,512]{1,0:T(8,128)(2,1)S(1)} %collective-permute-done.other_ref, f32[512,1024]{1,0:T(8,128)S(1)} %get-tuple-element.15.gate_in, f32[512,1024]{1,0:T(8,128)S(1)} %get-tuple-element.16.up_in, ...), custom_call_target="tpu_custom_call" | custom-call | flops 1610612736 | bytes 3145728 | tf_op jit(solution)/shard_map/hidden_part/pallas_call | solution.py:138
  62.4 0.1 collective-permute-start.1
  62.5 0.0 copy-done.2
  62.5 0.0 copy-done.3
  62.5 0.4 weigh.1.terms_ref
  62.9 0.0 copy-done.1
  62.9 0.7 keep_part.1
  63.6 0.0 copy-start.4
  63.6 0.8 collective-permute-done.1
  64.4 0.1 fusion
  64.5 35.5 %all_to_all.11 = bf16[64,8,512]{2,1,0:T(8,128)(2,1)S(1)} all-to-all(bf16[64,8,512]{2,1,0:T(8,128)(2,1)S(1)} %fusion), channel_id=1, replica_groups={{120,122,124,126,0,2,4,6,8,10,12,14,16,18,20,22,24,26,28,30,32,34,36,38..., dimensions={0} | all-to-all | bytes 1048576 | tf_op jit(solution)/shard_map/all_to_all | solution.py:213
  100.0 0.3 combine.1
  100.4 3.8 %collective-permute-start.2 = (f32[64,128]{1,0:T(8,128)S(1)}, f32[64,128]{1,0:T(8,128)S(1)}, u32[]{:S(2)}, u32[]{:S(2)}) collective-permute-start(f32[64,128]{1,0:T(8,128)S(1)} %get-tuple-element.24.square_ref), channel_id=1, source_target_pairs={{0,1},{1,0},{2,3},{3,2},{4,5},{5,4},{6,7},{7,6},{8,9},{9,8},{10,11... | collective-permute-start | bytes 98312 | tf_op jit(solution)/shard_map/ppermute | solution.py:210
  104.1 0.9 collective-permute-done.2.other_ref
  105.0 0.0 copy-done.4
  105.0 0.7 norm.1
Async XLA Ops:
  0.0 57.7 %copy-start = (bf16[1,1024,1024]{2,1,0:T(8,128)(2,1)S(1)}, bf16[1,1024,1024]{2,1,0:T(8,128)(2,1)}, u32[]{:S(2)}) copy-start(bf16[1,1024,1024]{2,1,0:T(8,128)(2,1)} %gate_ref.3) | copy-start | bytes 6291460
  53.9 6.4 %collective-permute-start = (bf16[512,512]{1,0:T(8,128)(2,1)S(1)}, bf16[512,512]{1,0:T(8,128)(2,1)S(1)}, u32[]{:S(2)}, u32[]{:S(2)}) collective-permute-start(bf16[512,512]{1,0:T(8,128)(2,1)S(1)} %bitcast.10), channel_id=1, source_target_pairs={{0,1},{1,0},{2,3},{3,2},{4,5},{5,4},{6,7},{7,6},{8,9},{9,8},{10,11... | collective-permute-start | bytes 1572872 | tf_op jit(solution)/shard_map/ppermute | solution.py:210
  60.3 2.2 %copy-start.2 = (s32[64,4]{0,1:T(4,128)S(1)}, s32[64,4]{0,1:T(4,128)}, u32[]{:S(2)}) copy-start(s32[64,4]{0,1:T(4,128)} %param.8) | copy-start | bytes 3076
  60.3 2.2 %copy-start.3 = (f32[64,4]{0,1:T(4,128)S(1)}, f32[64,4]{0,1:T(4,128)}, u32[]{:S(2)}) copy-start(f32[64,4]{0,1:T(4,128)} %param.9) | copy-start | bytes 3076
  60.3 2.5 %copy-start.1 = (bf16[1,1024,1024]{2,1,0:T(8,128)(2,1)S(1)}, bf16[1,1024,1024]{2,1,0:T(8,128)(2,1)}, u32[]{:S(2)}) copy-start(bf16[1,1024,1024]{2,1,0:T(8,128)(2,1)} %down_ref.1) | copy-start | bytes 6291460
  62.4 2.0 %collective-permute-start.1 = (bf16[512,512]{1,0:T(8,128)(2,1)S(1)}, bf16[512,512]{1,0:T(8,128)(2,1)S(1)}, u32[]{:S(2)}, u32[]{:S(2)}) collective-permute-start(bf16[512,512]{1,0:T(8,128)(2,1)S(1)} %get-tuple-element.22), channel_id=1, source_target_pairs={{0,1},{1,0},{2,3},{3,2},{4,5},{5,4},{6,7},{7,6},{8,9},{9,8},{10,11... | collective-permute-start | bytes 1572872 | tf_op jit(solution)/shard_map/ppermute | solution.py:210
  63.6 41.4 %copy-start.4 = (f32[512]{0:T(512)S(1)}, f32[512]{0:T(512)}, u32[]{:S(2)}) copy-start(f32[512]{0:T(512)} %param.13) | copy-start | bytes 6148
  100.4 4.6 %collective-permute-start.2 = (f32[64,128]{1,0:T(8,128)S(1)}, f32[64,128]{1,0:T(8,128)S(1)}, u32[]{:S(2)}, u32[]{:S(2)}) collective-permute-start(f32[64,128]{1,0:T(8,128)S(1)} %get-tuple-element.24.square_ref), channel_id=1, source_target_pairs={{0,1},{1,0},{2,3},{3,2},{4,5},{5,4},{6,7},{7,6},{8,9},{9,8},{10,11... | collective-permute-start | bytes 98312 | tf_op jit(solution)/shard_map/ppermute | solution.py:210
